TPU v7x, 32 devices: a whole 2x2x4 slice. The times are simulated.
32 devices in a mesh: fs: 8 (over z, x), tp: 4 (over y, core).
Axes of the slice: x: 2, y: 2, z: 4, core: 2. Of those that a mesh axis runs over, the one named last changes fastest.
Arguments:
- inputs: bfloat16 [1024, 2048], P('fs', 'tp'), may hold values from -6 to 6
- query_grad: bfloat16 [1024, 1024], P('fs', 'tp'), may hold values from -6 to 6
- forget_grad: bfloat16 [1024, 1024], P('fs', 'tp'), may hold values from -6 to 6
- forget_pre: bfloat16 [1024, 1024], P('fs', 'tp'), may hold values from -8 to 8
- lower_bound: float32 [1024], P('tp'), may hold values from 0.1 to 0.9
- query_weight: float32 [2048, 1024], P('fs', 'tp'), may hold values from -0.125 to 0.125
- forget_weight: float32 [2048, 1024], P('fs', 'tp'), may hold values from -0.125 to 0.125
- query_moment: float32 [2048, 1024], P('fs', 'tp'), may hold values from -6 to 6
- forget_moment: float32 [2048, 1024], P('fs', 'tp'), may hold values from -6 to 6
- query_rows: float32 [2048, 2048], P('fs'), may hold values from -0.6 to 0.6
- forget_rows: float32 [2048, 2048], P('fs'), may hold values from -0.6 to 0.6
- query_cols: float32 [8, 128, 128], P('tp'), may hold values from -0.6 to 0.6
- forget_cols: float32 [8, 128, 128], P('tp'), may hold values from -0.6 to 0.6
- query_row_root: bfloat16 [2048, 2048], P('fs'), may hold values from -2 to 2, as said below
- forget_row_root: bfloat16 [2048, 2048], P('fs'), may hold values from -2 to 2, as said below
- query_col_root: bfloat16 [8, 128, 128], P('tp'), may hold values from -2 to 2, as said below
- forget_col_root: bfloat16 [8, 128, 128], P('tp'), may hold values from -2 to 2, as said below
Outputs:
- query_master: float32 [2048, 1024], P('fs', 'tp')
- forget_master: float32 [2048, 1024], P('fs', 'tp')
- query_copy: bfloat16 [2048, 1024], P('fs', 'tp')
- forget_copy: bfloat16 [2048, 1024], P('fs', 'tp')
- query_step: float32 [2048, 1024], P('fs', 'tp')
- forget_step: float32 [2048, 1024], P('fs', 'tp')
- query_moment_next: float32 [2048, 1024], P('fs', 'tp')
- forget_moment_next: float32 [2048, 1024], P('fs', 'tp')
- query_rows_next: float32 [2048, 2048], P('fs')
- forget_rows_next: float32 [2048, 2048], P('fs')
- query_cols_next: float32 [8, 128, 128], P('tp')
- forget_cols_next: float32 [8, 128, 128], P('tp')
Inputs may be any that keep to these rules, and one draw needn't show every extreme that they name: `query_row_root`: diagonal entries 0.5 to 1.5, the others of order 2048 ** -0.5. `forget_row_root`: diagonal entries 0.5 to 1.5, the others of order 2048 ** -0.5. `query_col_root`: diagonal entries 0.5 to 1.5, the others of order 128 ** -0.5. `forget_col_root`: diagonal entries 0.5 to 1.5, the others of order 128 ** -0.5.
All inputs are finite; a program needn't handle non-finite values.
Results may differ from a plain program's by a relative error of at most 0.005.
Values may be sent and summed in bfloat16 or wider, within the bound.
A program may use at most 64 MiB of HBM per device.

v0:
```python
import jax
import jax.numpy as jnp
from jax import lax
from jax.sharding import PartitionSpec as P

D = 2048
HW = 1024
HEAD = 128


stat_decay = 0.9
moment_decay = 0.9
learn_rate = 0.02
highest = lax.Precision.HIGHEST


def fold_one(carry_state, shard_piece, offset, root_mine, grad_mine):
    left_sum, outer_rows, column_total = carry_state
    row_count, col_width = shard_piece.shape
    left_sum = left_sum + jnp.dot(root_mine, shard_piece, precision=highest)
    outer_piece = lax.dot_general(
        grad_mine, shard_piece, (((1,), (1,)), ((), ())), precision=highest
    )
    outer_rows = lax.dynamic_update_slice_in_dim(outer_rows, outer_piece, offset, 1)
    by_head = shard_piece.reshape(row_count, col_width // HEAD, HEAD)
    column_total = column_total + jnp.einsum("rhi,rhj->hij", by_head, by_head, precision=highest)
    return (left_sum, outer_rows, column_total)


def finish(weight, moment, rows, cols, col_root, left_sum, outer_rows, column_total, square):
    norm_scale = jnp.sqrt(D * HW / (square + 1.0))
    scale_twice = norm_scale * norm_scale
    rows_next = stat_decay * rows + (1.0 - stat_decay) / HW * scale_twice * outer_rows
    cols_next = stat_decay * cols + (1.0 - stat_decay) / D * scale_twice * column_total
    shard_rows, col_width = left_sum.shape
    shaped = left_sum.reshape(shard_rows, col_width // HEAD, HEAD)
    precond = norm_scale * jnp.einsum(
        "rhi,hij->rhj", shaped, col_root.astype(jnp.float32), precision=highest
    ).reshape(shard_rows, col_width)
    moment_next = moment_decay * moment + (1.0 - moment_decay) * precond
    update_step = moment_decay * moment_next + (1.0 - moment_decay) * precond
    master = weight - learn_rate * update_step
    return (master, master.astype(jnp.bfloat16), update_step, moment_next, rows_next, cols_next)


def on_device(
    inputs,
    query_grad,
    forget_grad,
    forget_pre,
    lower_bound,
    query_weight,
    forget_weight,
    query_moment,
    forget_moment,
    query_rows,
    forget_rows,
    query_cols,
    forget_cols,
    query_row_root,
    forget_row_root,
    query_col_root,
    forget_col_root,
):
    sigma_gate = jax.nn.sigmoid(forget_pre.astype(jnp.float32))
    forget_cot = (
        forget_grad.astype(jnp.float32) * (1.0 - lower_bound) * sigma_gate * (1.0 - sigma_gate)
    ).astype(jnp.bfloat16)
    gathered = lax.all_gather(inputs, "tp", axis=1, tiled=True)
    shard_rows, col_width = query_weight.shape
    heads_here = col_width // HEAD
    row_roots = (query_row_root.astype(jnp.float32), forget_row_root.astype(jnp.float32))
    empty = (
        jnp.zeros((shard_rows, col_width), jnp.float32),
        jnp.zeros((shard_rows, D), jnp.float32),
        jnp.zeros((heads_here, HEAD, HEAD), jnp.float32),
    )
    joined = jnp.concatenate([query_grad, forget_cot], axis=1)
    summed = lax.psum_scatter(
        lax.dot_general(
            gathered, joined, (((0,), (0,)), ((), ())), preferred_element_type=jnp.float32
        ),
        "fs",
        scatter_dimension=0,
        tiled=True,
    )
    gradients = (summed[:, :col_width], summed[:, col_width:])
    offset = jnp.int32(0)
    results = (
        fold_one(
            empty,
            lax.all_gather(gradients[0].astype(jnp.bfloat16), "fs", axis=0, tiled=True).astype(
                jnp.float32
            ),
            offset,
            row_roots[0],
            gradients[0],
        ),
        fold_one(
            empty,
            lax.all_gather(gradients[1].astype(jnp.bfloat16), "fs", axis=0, tiled=True).astype(
                jnp.float32
            ),
            offset,
            row_roots[1],
            gradients[1],
        ),
    )
    query_trace = jnp.sum(jnp.diagonal(results[0][2], axis1=1, axis2=2))
    forget_trace = jnp.sum(jnp.diagonal(results[1][2], axis1=1, axis2=2))
    query_outer, forget_outer, query_square, forget_square = (
        lax.psum(results[0][1].astype(jnp.bfloat16), "tp").astype(jnp.float32),
        lax.psum(results[1][1].astype(jnp.bfloat16), "tp").astype(jnp.float32),
        lax.psum(query_trace.astype(jnp.bfloat16), "tp").astype(jnp.float32),
        lax.psum(forget_trace.astype(jnp.bfloat16), "tp").astype(jnp.float32),
    )
    query_out = finish(
        query_weight,
        query_moment,
        query_rows,
        query_cols,
        query_col_root,
        results[0][0],
        query_outer,
        results[0][2],
        query_square,
    )
    forget_out = finish(
        forget_weight,
        forget_moment,
        forget_rows,
        forget_cols,
        forget_col_root,
        results[1][0],
        forget_outer,
        results[1][2],
        forget_square,
    )
    return (
        query_out[0],
        forget_out[0],
        query_out[1],
        forget_out[1],
        query_out[2],
        forget_out[2],
        query_out[3],
        forget_out[3],
        query_out[4],
        forget_out[4],
        query_out[5],
        forget_out[5],
    )


def solution(mesh):
    in_specs = (
        P("fs", "tp"),
        P("fs", "tp"),
        P("fs", "tp"),
        P("fs", "tp"),
        P("tp"),
        P("fs", "tp"),
        P("fs", "tp"),
        P("fs", "tp"),
        P("fs", "tp"),
        P("fs", None),
        P("fs", None),
        P("tp", None, None),
        P("tp", None, None),
        P("fs", None),
        P("fs", None),
        P("tp", None, None),
        P("tp", None, None),
    )
    out_specs = (
        P("fs", "tp"),
        P("fs", "tp"),
        P("fs", "tp"),
        P("fs", "tp"),
        P("fs", "tp"),
        P("fs", "tp"),
        P("fs", "tp"),
        P("fs", "tp"),
        P("fs", None),
        P("fs", None),
        P("tp", None, None),
        P("tp", None, None),
    )
    return jax.shard_map(
        on_device, mesh=mesh, in_specs=in_specs, out_specs=out_specs, check_vma=False
    )
```

profile of v0, /device:TPU:0, one launch (start us, length us, event | category | flops | bytes accessed | tf_op | source)
XLA Modules:
  0.0 288.4 jit_solution(1991709599089156850)
XLA Ops:
  7.2 0.8 broadcast_subtract_fusion
  8.0 8.9 %all_gather.9 = bf16[128,2048]{1,0:T(8,128)(2,1)S(1)} all-gather(bf16[128,512]{1,0:T(8,128)(2,1)} %param.17), channel_id=1, replica_groups=mesh['fs'=8,'tp'=4] {'tp'}, dimensions={1}, use_global_device_ids=true | all-gather | bytes 655360 | tf_op jit(solution)/shard_map/all_gather | solution.py:69
  16.9 0.9 multiply_convert_fusion
  17.8 3.5 %convolution_bitcast_fusion = f32[2048,512]{0,1:T(8,128)} fusion(bf16[128,2048]{1,0:T(8,128)(2,1)S(1)} %all_gather.9, bf16[128,256]{1,0:T(8,128)(2,1)S(1)} %multiply_convert_fusion, bf16[128,256]{1,0:T(8,128)(2,1)} %param.18), kind=kOutput, calls=%fused_computation.2 | convolution fusion | flops 268697600 | bytes 4849664 | tf_op jit(solution)/shard_map/dot_general | solution.py:80
  21.4 89.6 %reduce-scatter.2.cloned.1.call-done = f32[256,512]{0,1:T(8,128)} async-done(((f32[2048,512]{0,1:T(8,128)}), f32[256,512]{0,1:T(8,128)}) %reduce-scatter.2.cloned.1.call-update) | async-done | bytes 524304 | tf_op jit(solution)/shard_map/reduce_scatter | solution.py:79
  111.0 1.8 fusion.10
  112.8 0.7 all-gather.5.cloned.1.call-update
  113.6 39.1 %all-gather.3.cloned.1.call-done = bf16[2048,256]{0,1:T(8,128)(2,1)} async-done(((bf16[256,256]{0,1:T(8,128)(2,1)}), bf16[2048,256]{0,1:T(8,128)(2,1)}) %all-gather.3.cloned.1.call-update) | async-done | bytes 1048592 | tf_op jit(solution)/shard_map/all_gather | solution.py:92
  152.7 2.0 fusion.11
  154.7 39.1 %all-gather.5.cloned.1.call-done = bf16[2048,256]{0,1:T(8,128)(2,1)} async-done(((bf16[256,256]{0,1:T(8,128)(2,1)}), bf16[2048,256]{0,1:T(8,128)(2,1)}) %all-gather.5.cloned.1.call-update) | async-done | bytes 1048592 | tf_op jit(solution)/shard_map/all_gather | solution.py:101
  193.8 2.1 fusion.13
  195.9 4.6 %copy.36 = f32[2,128,128]{0,2,1:T(8,128)} copy(f32[2,128,128]{2,1,0:T(8,128)S(1)} %fusion.13) | data formatting | bytes 262144 | tf_op jit(solution)/shard_map/rhi,rhj->hij/dot_general | solution.py:26
  200.5 4.6 %copy.30 = f32[2,128,128]{0,2,1:T(8,128)} copy(f32[2,128,128]{2,1,0:T(8,128)S(1)} %fusion.11) | data formatting | bytes 262144 | tf_op jit(solution)/shard_map/rhi,rhj->hij/dot_general | solution.py:26
  205.1 1.8 gather_fusion.1
  206.9 1.8 gather_fusion
  208.6 0.6 reduce_sum.19
  209.3 0.6 reduce_sum.18
  209.9 6.7 %all-reduce = (bf16[]{:T(256)}, bf16[]{:T(256)}) all-reduce(bf16[]{:T(256)} %reduce_sum.18, bf16[]{:T(256)} %reduce_sum.19), channel_id=1, replica_groups=mesh['fs'=8,'tp'=4] {'tp'}, use_global_device_ids=true, to_apply=%region_2.3 | all-reduce | flops 2 | bytes 8 | tf_op jit(solution)/shard_map/psum | solution.py:114
  218.1 0.5 fusion.14
  218.6 1.0 fusion
  219.6 1.8 copy.39
  221.4 3.0 %convolution_convert_fusion.1 = bf16[256,2048]{1,0:T(8,128)(2,1)} fusion(bf16[2048,256]{0,1:T(8,128)(2,1)S(1)} %copy-done.1, f32[256,512]{0,1:T(8,128)} %reduce-scatter.2.cloned.1.call-done), kind=kOutput, calls=%fused_computation.4 | convolution fusion | flops 1611137024 | bytes 2359296 | tf_op jit(solution)/shard_map/dot_general | solution.py:21
  224.4 2.0 convolution_convert_fusion
  226.4 1.2 copy-done.5
  227.6 0.5 fusion.12
  228.1 0.4 copy-done.8
  228.5 0.3 fusion.1
  228.8 0.8 copy.33
  229.6 1.8 multiply_add_fusion.6
  231.4 2.6 fusion.8
  234.0 42.8 %all-reduce.4.cloned.1.call-done = (bf16[256,2048]{1,0:T(8,128)(2,1)}, bf16[256,2048]{1,0:T(8,128)(2,1)}) async-done(((bf16[256,2048]{1,0:T(8,128)(2,1)}, bf16[256,2048]{1,0:T(8,128)(2,1)}), (bf16[256,2048]{1,0:T(8,128)(2,1)}, bf16[256,2048]{1,0:T(8,128)(2,1)})) %all-reduce.4.cloned.1.call-update) | async-done | bytes 2097168 | tf_op jit(solution)/shard_map/psum | solution.py:112
  276.8 5.0 %multiply_add_fusion = (f32[256,2048]{1,0:T(8,128)}, f32[256,2048]{1,0:T(8,128)}) fusion(bf16[256,2048]{1,0:T(8,128)(2,1)} %get-tuple-element.15, f32[256,2048]{1,0:T(8,128)S(1)} %copy-done.3, f32[]{:T(128)S(6)} %mul.149, bf16[256,2048]{1,0:T(8,128)(2,1)} %get-tuple-element.14, f32[]{:T(128)S(6)} %mul.144, f32[256,2048]{1,0:T(8,128)} %param.26), kind=kLoop, calls=%fused_computation.5 | loop fusion | flops 4194304 | bytes 10485768 | tf_op jit(solution)/shard_map/add | solution.py:33
  (24 shorter events, 0.3 us)
Async XLA Ops:
  7.2 210.9 %copy-start = (bf16[256,2048]{1,0:T(8,128)(2,1)S(1)}, bf16[256,2048]{1,0:T(8,128)(2,1)}, u32[]{:S(2)}) copy-start(bf16[256,2048]{1,0:T(8,128)(2,1)} %param.31) | copy-start | bytes 3145732
  7.2 103.8 %reduce-scatter.2.cloned.1.call-start = ((), (), s32[]{:S(2)}) async-start(), calls=%async_computation.1 | async-start | bytes 4718592 | tf_op jit(solution)/shard_map/reduce_scatter | solution.py:79
  21.3 131.3 %all-gather.3.cloned.1.call-start = ((), (), s32[]{:S(2)}) async-start(), calls=%async_computation.2 | async-start | bytes 1179648 | tf_op jit(solution)/shard_map/all_gather | solution.py:92
  112.8 81.0 %all-gather.5.cloned.1.call-start = ((), (), s32[]{:S(2)}) async-start(), calls=%async_computation.3 | async-start | bytes 1179648 | tf_op jit(solution)/shard_map/all_gather | solution.py:101
  113.5 163.3 %all-reduce.4.cloned.1.call-start = ((), (), s32[]{:S(2)}) async-start(), calls=%async_computation.4 | async-start | bytes 4194304 | tf_op jit(solution)/shard_map/psum | solution.py:112
  200.5 17.6 %copy-start.2 = (bf16[2048,256]{0,1:T(8,128)(2,1)S(1)}, bf16[2048,256]{0,1:T(8,128)(2,1)}, u32[]{:S(2)}) copy-start(bf16[2048,256]{0,1:T(8,128)(2,1)} %all-gather.5.cloned.1.call-done) | copy-start | bytes 3145732
  205.1 16.3 %copy-start.1 = (bf16[2048,256]{0,1:T(8,128)(2,1)S(1)}, bf16[2048,256]{0,1:T(8,128)(2,1)}, u32[]{:S(2)}) copy-start(bf16[2048,256]{0,1:T(8,128)(2,1)} %all-gather.3.cloned.1.call-done) | copy-start | bytes 3145732
  209.3 9.3 %copy-start.7 = (bf16[2,128,128]{2,1,0:T(8,128)(2,1)S(1)}, bf16[2,128,128]{2,1,0:T(8,128)(2,1)}, u32[]{:S(2)}) copy-start(bf16[2,128,128]{2,1,0:T(8,128)(2,1)} %param.33) | copy-start | bytes 196612
  221.4 3.0 %copy-start.4 = (f32[256,512]{0,1:T(8,128)S(1)}, f32[256,512]{0,1:T(8,128)}, u32[]{:S(2)}) copy-start(f32[256,512]{0,1:T(8,128)} %reduce-scatter.2.cloned.1.call-done) | copy-start | bytes 1572868
  226.4 1.2 copy-start.5
  227.6 0.8 copy-start.8
  227.6 2.0 copy-start.6
  229.6 47.2 %copy-start.3 = (f32[256,2048]{1,0:T(8,128)S(1)}, f32[256,2048]{1,0:T(8,128)}, u32[]{:S(2)}) copy-start(f32[256,2048]{1,0:T(8,128)} %param.27) | copy-start | bytes 6291460
Sparse Core Ops, SparseCore 0:
  21.5 89.4 reduce-scatter.1
  113.6 39.0 all-gather.2
  155.3 38.3 all-gather.4
  226.5 50.2 all-reduce.3
where the time goes:
time: 289 us; the launch traced here: 288 us
  waiting for transfers between devices  211 us (73%)
  local copies, waits for them, and re-layouts  18.7 us (6%)
  blocking collectives  15.6 us (5%)
  between operations  15.3 us (5%)
  matrix products  14.9 us (5%)
  other arithmetic  12.4 us (4%)
    reduce_scatter x1, waiting for transfers between devices, on_device(): lax.psum_scatter(lax.dot_general(gathered, joined, (((0,), (0,)), ((), ()...  89.6 us
    psum x1, waiting for transfers between devices, on_device(): lax.psum(results[0][1].astype(jnp.bfloat16), 'tp').astype(jnp.float32)  42.8 us
    all_gather x1, waiting for transfers between devices, on_device(): lax.all_gather(gradients[0].astype(jnp.bfloat16), 'fs', axis=0, tiled=True)  39.1 us
    all_gather x1, waiting for transfers between devices, on_device(): lax.all_gather(gradients[1].astype(jnp.bfloat16), 'fs', axis=0, tiled=True)  39.1 us
    dot_general x2, local copies, waits for them, and re-layouts, fold_one(): jnp.einsum('rhi,rhj->hij', by_head, by_head, precision=highest)  9.2 us
    all_gather x1, blocking collectives, on_device(): gathered = lax.all_gather(inputs, 'tp', axis=1, tiled=True)  8.87 us
    psum x1, blocking collectives, on_device(): lax.psum(query_trace.astype(jnp.bfloat16), 'tp').astype(jnp.float32)  6.7 us
  transfers between devices with their start and end apart: 4, of which 4 were waited for; matrix products, arithmetic and copies ran while one was open for 3% of the time, Pallas kernels for 0%

commit v1 on v0

--- a/solution.py
+++ b/solution.py
@@ -43,7 +43,7 @@
     return (master, master.astype(jnp.bfloat16), update_step, moment_next, rows_next, cols_next)
 
 
-def on_device(
+def reduce_plan(
     inputs,
     query_grad,
     forget_grad,
@@ -152,6 +152,104 @@
     )
 
 
+def to_bf16(value):
+    return value.astype(jnp.bfloat16)
+
+
+def wide_dot(left, right, dims):
+    return lax.dot_general(left, right, (dims, ((), ())), preferred_element_type=jnp.float32)
+
+
+def gather_blocks(tokens_block, cot_block):
+    axes = ("fs", "tp")
+    sizes = (lax.axis_size("fs"), lax.axis_size("tp"))
+    gathered = lax.all_gather(tokens_block, axes, axis=0, tiled=False)
+    cots = lax.all_gather(cot_block, axes, axis=0, tiled=False)
+    return (
+        gathered.reshape(sizes + tokens_block.shape),
+        cots.reshape(sizes + cot_block.shape),
+    )
+
+
+def whole(blocks):
+    shards, parts, rows, cols = blocks.shape
+    return blocks.transpose(0, 2, 1, 3).reshape(shards * rows, parts * cols)
+
+
+def update(weight, moment, rows, cols, row_root, col_root, inputs_all, cot_all):
+    gradient = wide_dot(inputs_all, cot_all, ((0,), (0,)))
+    square = jnp.sum(gradient * gradient)
+    norm_scale = jnp.sqrt(gradient.shape[0] * gradient.shape[1] / (square + 1.0))
+    scale_twice = norm_scale * norm_scale
+    narrow = to_bf16(gradient)
+    shard_rows, col_width = weight.shape
+    mine = lax.dynamic_slice_in_dim(narrow, lax.axis_index("fs") * shard_rows, shard_rows, 0)
+    own = lax.dynamic_slice_in_dim(narrow, lax.axis_index("tp") * col_width, col_width, 1)
+    outer = wide_dot(mine, narrow, ((1,), (1,)))
+    rows_next = stat_decay * rows + (1.0 - stat_decay) / HW * scale_twice * outer
+    heads = col_width // HEAD
+    left_sum = to_bf16(wide_dot(row_root, own, ((1,), (0,))))
+    column_parts = []
+    precond_parts = []
+    for head in range(heads):
+        part = own[:, head * HEAD : (head + 1) * HEAD]
+        column_parts.append(wide_dot(part, part, ((0,), (0,))))
+        precond_parts.append(
+            wide_dot(left_sum[:, head * HEAD : (head + 1) * HEAD], col_root[head], ((1,), (0,)))
+        )
+    cols_next = stat_decay * cols + (1.0 - stat_decay) / D * scale_twice * jnp.stack(column_parts)
+    precond = norm_scale * jnp.concatenate(precond_parts, axis=1)
+    moment_next = moment_decay * moment + (1.0 - moment_decay) * precond
+    update_step = moment_decay * moment_next + (1.0 - moment_decay) * precond
+    master = weight - learn_rate * update_step
+    return (master, to_bf16(master), update_step, moment_next, rows_next, cols_next)
+
+
+def gather_plan(
+    inputs,
+    query_grad,
+    forget_grad,
+    forget_pre,
+    lower_bound,
+    query_weight,
+    forget_weight,
+    query_moment,
+    forget_moment,
+    query_rows,
+    forget_rows,
+    query_cols,
+    forget_cols,
+    query_row_root,
+    forget_row_root,
+    query_col_root,
+    forget_col_root,
+):
+    sigma_gate = jax.nn.sigmoid(forget_pre.astype(jnp.float32))
+    forget_cot = to_bf16(
+        forget_grad.astype(jnp.float32) * (1.0 - lower_bound) * sigma_gate * (1.0 - sigma_gate)
+    )
+    width = query_grad.shape[1]
+    inputs_all, cots = gather_blocks(inputs, jnp.concatenate([query_grad, forget_cot], axis=1))
+    inputs_all = whole(inputs_all)
+    query_out = update(
+        query_weight, query_moment, query_rows, query_cols, query_row_root, query_col_root,
+        inputs_all, whole(cots[..., :width]),
+    )
+    forget_out = update(
+        forget_weight, forget_moment, forget_rows, forget_cols, forget_row_root, forget_col_root,
+        inputs_all, whole(cots[..., width:]),
+    )
+    return tuple(piece for pair in zip(query_out, forget_out) for piece in pair)
+
+
+def on_device(*args):
+    token_count = args[0].shape[0] * lax.axis_size("fs")
+    feature_count = args[0].shape[1] * lax.axis_size("tp")
+    if token_count <= feature_count:
+        return gather_plan(*args)
+    return reduce_plan(*args)
+
+
 def solution(mesh):
     in_specs = (
         P("fs", "tp"),

time: 289 us -> 208 us (0.72)
  waiting for transfers between devices: 211 us -> 114 us
  local copies, waits for them, and re-layouts: 18.7 us -> 39.1 us
  blocking collectives: 15.6 us -> 0 us
  matrix products: 14.9 us -> 29.8 us
  other arithmetic: 12.4 us -> 8.63 us
    reduce_scatter x1 -> x0, waiting for transfers between devices: 89.6 us -> none  [on_device(): lax.psum_scatter(lax.dot_general(gathered, joined, (((0,), (0,)), ((), ()...]
    psum x1 -> x0, waiting for transfers between devices: 42.8 us -> none  [on_device(): lax.psum(results[0][1].astype(jnp.bfloat16), 'tp').astype(jnp.float32)]
    all_gather x2, waiting for transfers between devices: 78.2 us -> 113 us  [the longest x1 58.2 us: gather_blocks(): cots = lax.all_gather(cot_block, axes, axis=0, tiled=False)]
    unnamed x18 -> x48, local copies, waits for them, and re-layouts: 1.59 us -> 27.4 us
    dot_general x9 -> x14, matrix products: 14.9 us -> 29.8 us  [wide_dot(): lax.dot_general(left, right, (dims, ((), ())), preferred_element_type=jnp...]
    dot_general x2 -> x0, local copies, waits for them, and re-layouts: 9.2 us -> none  [fold_one(): jnp.einsum('rhi,rhj->hij', by_head, by_head, precision=highest)]
    all_gather x1 -> x0, blocking collectives: 8.87 us -> none  [on_device(): gathered = lax.all_gather(inputs, 'tp', axis=1, tiled=True)]
    reshape x0 -> x1, local copies, waits for them, and re-layouts: none -> 7.63 us  [gather_blocks(): gathered.reshape(sizes + tokens_block.shape)]
  transfers between devices with their start and end apart: 4 -> 2, of which waited for: 4 -> 2; matrix products, arithmetic and copies ran while one was open for 3% -> 7% of each run, Pallas kernels for 0% -> 0%
where the time goes in v1:
time: 208 us; the launch traced here: 207 us
  waiting for transfers between devices  114 us (55%)
  local copies, waits for them, and re-layouts  39.1 us (19%)
  matrix products  29.8 us (14%)
  between operations  15.7 us (8%)
  other arithmetic  8.63 us (4%)
    all_gather x1, waiting for transfers between devices, gather_blocks(): cots = lax.all_gather(cot_block, axes, axis=0, tiled=False)  58.2 us
    all_gather x1, waiting for transfers between devices, gather_blocks(): gathered = lax.all_gather(tokens_block, axes, axis=0, tiled=False)  55.1 us
    dot_general x14, matrix products, wide_dot(): lax.dot_general(left, right, (dims, ((), ())), preferred_element_type=jnp...  29.8 us
    unnamed x48, local copies, waits for them, and re-layouts  27.4 us
    reshape x1, local copies, waits for them, and re-layouts, gather_blocks(): gathered.reshape(sizes + tokens_block.shape)  7.63 us
    convert_element_type x3, other arithmetic, to_bf16(): return value.astype(jnp.bfloat16)  5.02 us
  transfers between devices with their start and end apart: 2, of which 2 were waited for; matrix products, arithmetic and copies ran while one was open for 7% of the time, Pallas kernels for 0%

profile of v1, /device:TPU:0, one launch (start us, length us, event | category | flops | bytes accessed | tf_op | source)
XLA Modules:
  0.0 207.3 jit_solution(1343497522538063659)
XLA Ops:
  8.0 0.9 multiply_convert_fusion
  8.9 1.5 pad_maximum_fusion
  11.2 1.8 copy.45
  13.0 1.8 copy.47
  14.8 1.1 copy.41
  15.9 1.8 copy.44
  17.7 58.2 %all-gather.5.cloned.1.call-done = bf16[4096,512]{1,0:T(8,128)(2,1)} async-done(((bf16[128,512]{1,0:T(8,128)(2,1)}), bf16[4096,512]{1,0:T(8,128)(2,1)}) %all-gather.5.cloned.1.call-update) | async-done | bytes 4194320 | tf_op jit(solution)/shard_map/all_gather | solution.py:167
  75.8 3.9 %fusion.48 = (bf16[8,4,128,256]{3,2,1,0:T(8,128)(2,1)}, bf16[8,4,128,256]{3,2,1,0:T(8,128)(2,1)S(1)}) fusion(bf16[8,4,128,512]{3,2,1,0:T(8,128)(2,1)} %bitcast.68), kind=kLoop, calls=%fused_computation.73 | loop fusion | bytes 8388608 | tf_op jit(solution)/shard_map/slice | solution.py:240
  79.7 4.3 %copy.57 = bf16[8,4,128,256]{2,0,3,1:T(8,128)(2,1)} copy(bf16[8,4,128,256]{3,2,1,0:T(8,128)(2,1)} %get-tuple-element.46) | data formatting | bytes 4194304
  84.0 55.1 %all-gather.7.cloned.1.call-done = bf16[4096,512]{1,0:T(8,128)(2,1)} async-done(((bf16[128,512]{1,0:T(8,128)(2,1)}), bf16[4096,512]{1,0:T(8,128)(2,1)}) %all-gather.7.cloned.1.call-update) | async-done | bytes 4194320 | tf_op jit(solution)/shard_map/all_gather | solution.py:166
  139.1 7.6 %copy.43 = bf16[8,4,128,512]{2,0,3,1:T(8,128)(2,1)} copy(bf16[8,4,128,512]{3,2,1,0:T(8,128)(2,1)} %bitcast.69) | data formatting | bytes 8388608 | tf_op jit(solution)/shard_map/reshape | solution.py:169
  146.7 2.6 %copy.56 = bf16[8,4,128,256]{2,0,3,1:T(8,128)(2,1)} copy(bf16[8,4,128,256]{3,2,1,0:T(8,128)(2,1)S(1)} %get-tuple-element.47) | data formatting | bytes 4194304
  149.3 8.4 %multiply_reduce_fusion = (f32[]{:T(128)}, bf16[1024,2048]{1,0:T(8,128)(2,1)S(1)}) fusion(bf16[256,8,8,128]{3,2,1,0:T(8,128)(2,1)} %bitcast.70, bf16[128,8,8,128]{3,2,1,0:T(8,128)(2,1)} %bitcast.72), kind=kOutput, calls=%fused_computation | convolution fusion | flops 4301258752 | bytes 10485764 | tf_op jit(solution)/shard_map/dot_general | solution.py:160
  157.7 6.2 %multiply_reduce_fusion.1 = (f32[]{:T(128)}, bf16[1024,2048]{1,0:T(8,128)(2,1)S(1)}) fusion(bf16[256,8,8,128]{3,2,1,0:T(8,128)(2,1)S(1)} %bitcast.71, bf16[128,8,8,128]{3,2,1,0:T(8,128)(2,1)S(1)} %bitcast.73), kind=kOutput, calls=%fused_computation.1 | convolution fusion | flops 4301258752 | bytes 10485764 | tf_op jit(solution)/shard_map/dot_general | solution.py:160
  164.1 0.9 convolution_bitcast_fusion
  165.0 0.9 convolution_bitcast_fusion.1
  165.9 0.9 convolution_bitcast_fusion.2
  166.9 0.9 convolution_bitcast_fusion.3
  168.3 0.9 fusion.26
  170.7 0.9 fusion.32
  173.1 2.1 %fusion.46 = (bf16[256,256]{0,1:T(8,128)(2,1)}, f32[256,256]{0,1:T(8,128)}, f32[256,256]{0,1:T(8,128)}, f32[256,256]{0,1:T(8,128)}) fusion(f32[256,256]{0,1:T(8,128)} %copy.47, f32[256,128]{0,1:T(8,128)} %fusion.26, f32[256,128]{0,1:T(8,128)} %fusion.28, f32[]{:T(128)S(6)} %sqrt.7, f32[256,256]{0,1:T(8,128)} %copy.45), kind=kLoop, calls=%fused_computation.71 | loop fusion | flops 655360 | bytes 1703940 | tf_op jit(solution)/shard_map/convert_element_type | solution.py:156
  175.2 1.8 copy.49
  177.0 1.8 copy.53
  178.8 1.8 copy.55
  180.6 1.7 copy.51
  182.2 2.0 fusion.47
  184.2 1.8 copy.48
  186.0 1.8 copy.52
  187.8 1.8 copy.54
  189.6 1.7 copy.50
  191.2 5.1 %fusion.7 = f32[256,2048]{1,0:T(8,128)} fusion(bf16[1024,2048]{1,0:T(8,128)(2,1)} %copy-done.1, f32[256,2048]{1,0:T(8,128)S(1)} %copy-done.5, f32[]{:T(128)S(6)} %mul.149, s32[]{:T(128)S(6)} %select_n.9), kind=kOutput, calls=%fused_computation.11 | convolution fusion | flops 1075314688 | bytes 8912904 | tf_op jit(solution)/shard_map/dot_general | solution.py:160
  196.4 2.7 %fusion.6 = f32[256,2048]{1,0:T(8,128)} fusion(bf16[1024,2048]{1,0:T(8,128)(2,1)S(1)} %copy-done.3, f32[256,2048]{1,0:T(8,128)S(1)} %copy-done.6, f32[]{:T(128)S(6)} %mul.143, s32[]{:T(128)S(6)} %select_n.9), kind=kOutput, calls=%fused_computation.10 | convolution fusion | flops 1075314688 | bytes 8912904 | tf_op jit(solution)/shard_map/dot_general | solution.py:160
  (46 shorter events, 5.1 us)
Async XLA Ops:
  7.2 160.6 %copy-start = (bf16[256,2048]{1,0:T(8,128)(2,1)S(1)}, bf16[256,2048]{1,0:T(8,128)(2,1)}, u32[]{:S(2)}) copy-start(bf16[256,2048]{1,0:T(8,128)(2,1)} %param.31) | copy-start | bytes 3145732
  7.2 68.6 %all-gather.5.cloned.1.call-start = ((), (), s32[]{:S(2)}) async-start(), calls=%async_computation | async-start | bytes 4325376 | tf_op jit(solution)/shard_map/all_gather | solution.py:167
  10.5 128.7 %all-gather.7.cloned.1.call-start = ((), (), s32[]{:S(2)}) async-start(), calls=%async_computation.1 | async-start | bytes 4325376 | tf_op jit(solution)/shard_map/all_gather | solution.py:166
  149.3 8.4 %copy-start.4 = (bf16[8,4,128,512]{2,0,3,1:T(8,128)(2,1)S(1)}, bf16[8,4,128,512]{2,0,3,1:T(8,128)(2,1)}, u32[]{:S(2)}) copy-start(bf16[8,4,128,512]{2,0,3,1:T(8,128)(2,1)} %copy.43) | copy-start | bytes 12582916
  149.3 8.4 %copy-start.7 = (bf16[8,4,128,256]{2,0,3,1:T(8,128)(2,1)S(1)}, bf16[8,4,128,256]{2,0,3,1:T(8,128)(2,1)}, u32[]{:S(2)}) copy-start(bf16[8,4,128,256]{2,0,3,1:T(8,128)(2,1)} %copy.56) | copy-start | bytes 6291460
  157.7 10.1 %copy-start.1 = (bf16[1024,2048]{1,0:T(8,128)(2,1)}, bf16[1024,2048]{1,0:T(8,128)(2,1)S(1)}, u32[]{:S(2)}) copy-start(bf16[1024,2048]{1,0:T(8,128)(2,1)S(1)} %get-tuple-element.43) | copy-start | bytes 12582916
  163.9 6.1 %copy-start.2 = (bf16[1024,2048]{1,0:T(8,128)(2,1)}, bf16[1024,2048]{1,0:T(8,128)(2,1)S(1)}, u32[]{:S(2)}) copy-start(bf16[1024,2048]{1,0:T(8,128)(2,1)S(1)} %get-tuple-element.45) | copy-start | bytes 12582916
  163.9 4.3 %copy-start.11 = (bf16[2,128,128]{2,1,0:T(8,128)(2,1)S(1)}, bf16[2,128,128]{2,1,0:T(8,128)(2,1)}, u32[]{:S(2)}) copy-start(bf16[2,128,128]{2,1,0:T(8,128)(2,1)} %param.33) | copy-start | bytes 196612
  163.9 6.1 %copy-start.8 = (bf16[256,2048]{1,0:T(8,128)(2,1)S(1)}, bf16[256,2048]{1,0:T(8,128)(2,1)}, u32[]{:S(2)}) copy-start(bf16[256,2048]{1,0:T(8,128)(2,1)} %param.30) | copy-start | bytes 3145732
  164.1 6.4 %copy-start.12 = (bf16[2,128,128]{2,1,0:T(8,128)(2,1)S(1)}, bf16[2,128,128]{2,1,0:T(8,128)(2,1)}, u32[]{:S(2)}) copy-start(bf16[2,128,128]{2,1,0:T(8,128)(2,1)} %param.32) | copy-start | bytes 196612
  170.5 20.7 %copy-start.5 = (f32[256,2048]{1,0:T(8,128)S(1)}, f32[256,2048]{1,0:T(8,128)}, u32[]{:S(2)}) copy-start(f32[256,2048]{1,0:T(8,128)} %param.27) | copy-start | bytes 6291460
  191.2 5.1 %copy-start.3 = (bf16[1024,2048]{1,0:T(8,128)(2,1)S(1)}, bf16[1024,2048]{1,0:T(8,128)(2,1)}, u32[]{:S(2)}) copy-start(bf16[1024,2048]{1,0:T(8,128)(2,1)} %copy-done.2) | copy-start | bytes 12582916
  191.2 5.1 %copy-start.6 = (f32[256,2048]{1,0:T(8,128)S(1)}, f32[256,2048]{1,0:T(8,128)}, u32[]{:S(2)}) copy-start(f32[256,2048]{1,0:T(8,128)} %param.26) | copy-start | bytes 6291460
  196.3 2.7 %copy-start.9 = (f32[2,128,128]{2,1,0:T(8,128)S(1)}, f32[2,128,128]{2,1,0:T(8,128)}, u32[]{:S(2)}) copy-start(f32[2,128,128]{2,1,0:T(8,128)} %param.29) | copy-start | bytes 393220
  196.3 2.7 %copy-start.13 = (f32[1,128,128]{2,1,0:T(8,128)S(1)}, f32[1,128,128]{2,1,0:T(8,128)}, u32[]{:S(2)}) copy-start(f32[1,128,128]{2,1,0:T(8,128)} %convolution_bitcast_fusion) | copy-start | bytes 196612
  196.4 2.7 %copy-start.14 = (f32[1,128,128]{2,1,0:T(8,128)S(1)}, f32[1,128,128]{2,1,0:T(8,128)}, u32[]{:S(2)}) copy-start(f32[1,128,128]{2,1,0:T(8,128)} %convolution_bitcast_fusion.1) | copy-start | bytes 196612
  196.4 3.4 %copy-start.10 = (f32[2,128,128]{2,1,0:T(8,128)S(1)}, f32[2,128,128]{2,1,0:T(8,128)}, u32[]{:S(2)}) copy-start(f32[2,128,128]{2,1,0:T(8,128)} %param.28) | copy-start | bytes 393220
  196.4 3.4 %copy-start.15 = (f32[1,128,128]{2,1,0:T(8,128)S(1)}, f32[1,128,128]{2,1,0:T(8,128)}, u32[]{:S(2)}) copy-start(f32[1,128,128]{2,1,0:T(8,128)} %convolution_bitcast_fusion.2) | copy-start | bytes 196612
  196.4 3.4 %copy-start.16 = (f32[1,128,128]{2,1,0:T(8,128)S(1)}, f32[1,128,128]{2,1,0:T(8,128)}, u32[]{:S(2)}) copy-start(f32[1,128,128]{2,1,0:T(8,128)} %convolution_bitcast_fusion.3) | copy-start | bytes 196612
Sparse Core Ops, SparseCore 0:
  11.4 64.3 all-gather.4
  78.7 60.3 all-gather.6

commit v2 on v0

--- a/solution.py
+++ b/solution.py
@@ -1,6 +1,10 @@
+import functools
+
 import jax
 import jax.numpy as jnp
 from jax import lax
+from jax.experimental import pallas as pl
+from jax.experimental.pallas import tpu as pltpu
 from jax.sharding import PartitionSpec as P
 
 D = 2048
@@ -12,6 +16,7 @@
 moment_decay = 0.9
 learn_rate = 0.02
 highest = lax.Precision.HIGHEST
+MESH = pl.DeviceIdType.MESH
 
 
 def fold_one(carry_state, shard_piece, offset, root_mine, grad_mine):
@@ -43,7 +48,7 @@
     return (master, master.astype(jnp.bfloat16), update_step, moment_next, rows_next, cols_next)
 
 
-def on_device(
+def reduce_plan(
     inputs,
     query_grad,
     forget_grad,
@@ -152,6 +157,313 @@
     )
 
 
+def to_bf16(value):
+    return value.astype(jnp.bfloat16)
+
+
+def wide_dot(left, right, dims):
+    return lax.dot_general(left, right, (dims, ((), ())), preferred_element_type=jnp.float32)
+
+
+def relay_kernel(
+    x_ref, g_ref, rq_ref, rf_ref, cq_ref, cf_ref,
+    sq_ref, sf_ref, pq_ref, pf_ref, kq_ref, kf_ref,
+    xs, gs, xt, grad, left, own_sem, send_sem, recv_sem,
+):
+    shards = xs.shape[0]
+    depth = shards // 2
+    block, span = x_ref.shape
+    fs = lax.axis_index("fs")
+    tp = lax.axis_index("tp")
+    z, px = lax.div(fs, 2), lax.rem(fs, 2)
+    py, pc = lax.div(tp, 2), lax.rem(tp, 2)
+    fs_other = fs + 1 - 2 * px
+    tp_other = tp + 2 - 4 * py
+    beside = {
+        "up": (fs + 2, tp),
+        "down": (fs - 2, tp),
+        "x": (fs_other, tp),
+        "y": (fs, tp_other),
+        "core": (fs, tp + 1 - 2 * pc),
+    }
+    has_up = z < depth - 1
+    has_down = z > 0
+
+    def guarded(cond, action):
+        if cond is None:
+            action()
+        else:
+            pl.when(cond)(action)
+
+    barrier = pltpu.get_barrier_semaphore()
+
+    def greet(name):
+        pl.semaphore_signal(barrier, inc=1, device_id=beside[name], device_id_type=MESH)
+
+    for name in ("x", "y", "core"):
+        greet(name)
+    guarded(has_up, lambda: greet("up"))
+    guarded(has_down, lambda: greet("down"))
+    pl.semaphore_wait(
+        barrier, 3 + jnp.where(has_up, 1, 0) + jnp.where(has_down, 1, 0)
+    )
+
+    slots = (xs, gs)
+    pending = []
+
+    def copy_of(kind, src, slot, name, number):
+        return pltpu.make_async_remote_copy(
+            src_ref=src,
+            dst_ref=slots[kind].at[slot[0], slot[1]],
+            send_sem=send_sem.at[number],
+            recv_sem=recv_sem.at[kind, slot[0], slot[1]],
+            device_id=beside[name],
+            device_id_type=MESH,
+        )
+
+    def send(kind, src, slot, name, cond=None):
+        number = len(pending)
+        build = functools.partial(copy_of, kind, src, slot, name, number)
+        guarded(cond, lambda: build().start())
+        pending.append((cond, build))
+
+    def arrive(kind, slot, cond=None):
+        here = slots[kind].at[slot[0], slot[1]]
+        guarded(cond, lambda: copy_of(kind, here, slot, "core", 0).wait_recv())
+
+    def forward(kind, slot, names, cond=None):
+        for name in names:
+            send(kind, slots[kind].at[slot[0], slot[1]], slot, name, cond)
+
+    own = (fs, tp)
+    orders = (("x", "y"), ("y", "x"))
+    sources = (x_ref, g_ref)
+
+    def crossed(kind, layer):
+        if kind == 0:
+            return (2 * layer + 1 - px, tp)
+        return (2 * layer + px, tp_other)
+
+    def lasts(kind, layer):
+        if kind == 0:
+            return ((2 * layer + px, tp_other), (2 * layer + 1 - px, tp_other))
+        return ((2 * layer + 1 - px, tp), (2 * layer + 1 - px, tp_other))
+
+    keep = [
+        pltpu.make_async_copy(sources[kind], slots[kind].at[fs, tp], own_sem.at[kind])
+        for kind in range(2)
+    ]
+    for kind in range(2):
+        send(kind, sources[kind], own, "up", has_up)
+        send(kind, sources[kind], own, "down", has_down)
+    for kind in range(2):
+        send(kind, sources[kind], own, orders[kind][0])
+    for kind in range(2):
+        send(kind, sources[kind], own, orders[kind][1])
+        send(kind, sources[kind], own, "core")
+        keep[kind].start()
+
+    def finals(stage):
+        for layer, cond in stage:
+            for kind in range(2):
+                for slot in lasts(kind, layer):
+                    arrive(kind, slot, cond)
+                    forward(kind, slot, ("core",), cond)
+
+    previous = None
+    for distance in range(depth):
+        stage = []
+        if distance == 0:
+            stage.append((z, None))
+        else:
+            stage.append((z - distance, z >= distance))
+            stage.append((z + distance, z + distance < depth))
+            for sign, (layer, cond) in zip((-1, 1), stage):
+                for kind in range(2):
+                    slot = (2 * layer + px, tp)
+                    arrive(kind, slot, cond)
+                    if sign < 0:
+                        onward, onto = "up", jnp.logical_and(cond, has_up)
+                    else:
+                        onward, onto = "down", jnp.logical_and(cond, has_down)
+                    if distance < depth - 1:
+                        forward(kind, slot, (onward,), onto)
+                    forward(kind, slot, orders[kind] + ("core",), cond)
+        for layer, cond in stage:
+            for kind in range(2):
+                slot = crossed(kind, layer)
+                arrive(kind, slot, cond)
+                forward(kind, slot, (orders[kind][1], "core"), cond)
+        if previous is not None:
+            finals(previous)
+        previous = stage
+    finals(previous)
+    for kind in range(2):
+        keep[kind].wait()
+    for layer in range(depth):
+        for across in range(2):
+            for part in range(2):
+                slot = (2 * layer + across, 2 * part + 1 - pc)
+                for kind in range(2):
+                    arrive(kind, slot)
+
+    @pl.loop(0, shards)
+    def _(shard):
+        lanes = pl.ds(pl.multiple_of(shard * block, block), block)
+        for part in range(xs.shape[1]):
+            xt[part * span : (part + 1) * span, lanes] = xs[shard, part].T
+
+    width = gs.shape[3] // 2
+    chunk = sq_ref.shape[0]
+    steps = xt.shape[0] // chunk
+    tokens = shards * block
+    own_lanes = pl.ds(pl.multiple_of(tp * width, width), width)
+    for which, (root, col_root, outer_ref, pre_ref, col_ref) in enumerate(
+        (
+            (rq_ref, cq_ref, sq_ref, pq_ref, kq_ref),
+            (rf_ref, cf_ref, sf_ref, pf_ref, kf_ref),
+        )
+    ):
+        def multiply(step, total, which=which):
+            rows = pl.ds(pl.multiple_of(step * chunk, chunk), chunk)
+            for part in range(gs.shape[1]):
+                cot = gs[:, part, :, which * width : (which + 1) * width].reshape(tokens, width)
+                piece = wide_dot(xt[rows, :], cot, ((1,), (0,)))
+                grad[rows, part * width : (part + 1) * width] = to_bf16(piece)
+                total = total + jnp.sum(piece * piece, axis=0, keepdims=True)
+            return total
+
+        total = lax.fori_loop(0, steps, multiply, jnp.zeros((1, width), jnp.float32))
+        square = jnp.sum(total, axis=1, keepdims=True)
+        scale_twice = float(grad.shape[0] * grad.shape[1]) / (square + 1.0)
+        norm_scale = jnp.sqrt(scale_twice)
+        left[...] = jnp.zeros_like(left)
+        col_ref[...] = jnp.zeros_like(col_ref)
+        mine = pl.ds(pl.multiple_of(fs * chunk, chunk), chunk)
+
+        @pl.loop(0, steps)
+        def _(step):
+            rows = pl.ds(pl.multiple_of(step * chunk, chunk), chunk)
+            outer = wide_dot(grad[mine, :], grad[rows, :], ((1,), (1,)))
+            outer_ref[:, rows] = to_bf16(
+                outer * ((1.0 - stat_decay) / grad.shape[1] * scale_twice)
+            )
+            part = grad[rows, own_lanes]
+            left[...] += wide_dot(root[:, rows], part, ((1,), (0,)))
+            for head in range(width // HEAD):
+                piece = part[:, head * HEAD : (head + 1) * HEAD]
+                col_ref[head] += wide_dot(piece, piece, ((0,), (0,)))
+
+        for head in range(width // HEAD):
+            lanes = slice(head * HEAD, (head + 1) * HEAD)
+            col_ref[head] = col_ref[head] * ((1.0 - stat_decay) / grad.shape[0] * scale_twice)
+            pre_ref[:, lanes] = norm_scale * wide_dot(
+                to_bf16(left[:, lanes]), col_root[head], ((1,), (0,))
+            )
+
+    for cond, build in pending:
+        guarded(cond, lambda build=build: build().wait_send())
+
+
+def relayed_products(x, cots, query_root, forget_root, query_col_root, forget_col_root):
+    shards, parts = lax.axis_size("fs"), lax.axis_size("tp")
+    block, span = x.shape
+    width = cots.shape[1] // 2
+    chunk, features = query_root.shape
+    depth = shards // 2
+    sends = 2 * (5 + 8 * (depth - 1) + 2 * (2 * depth - 1) + 2 * (2 * depth - 1))
+    f32 = jnp.float32
+    heads = query_col_root.shape
+    vmem = pl.BlockSpec(memory_space=pltpu.VMEM)
+    return pl.pallas_call(
+        relay_kernel,
+        out_shape=[
+            jax.ShapeDtypeStruct((chunk, features), jnp.bfloat16),
+            jax.ShapeDtypeStruct((chunk, features), jnp.bfloat16),
+            jax.ShapeDtypeStruct((chunk, width), f32),
+            jax.ShapeDtypeStruct((chunk, width), f32),
+            jax.ShapeDtypeStruct(heads, f32),
+            jax.ShapeDtypeStruct(heads, f32),
+        ],
+        in_specs=[vmem] * 6,
+        out_specs=[vmem] * 6,
+        scratch_shapes=[
+            pltpu.VMEM((shards, parts, block, span), jnp.bfloat16),
+            pltpu.VMEM((shards, parts, block, 2 * width), jnp.bfloat16),
+            pltpu.VMEM((features, shards * block), jnp.bfloat16),
+            pltpu.VMEM((features, parts * width), jnp.bfloat16),
+            pltpu.VMEM((chunk, width), f32),
+            pltpu.SemaphoreType.DMA((2,)),
+            pltpu.SemaphoreType.DMA((sends,)),
+            pltpu.SemaphoreType.DMA((2, shards, parts)),
+        ],
+        compiler_params=pltpu.CompilerParams(
+            collective_id=0, has_side_effects=True, vmem_limit_bytes=56 * 1024 * 1024
+        ),
+    )(x, cots, query_root, forget_root, query_col_root, forget_col_root)
+
+
+def finish_update(weight, moment, rows, cols, outer, precond, column):
+    rows_next = stat_decay * rows + outer.astype(jnp.float32)
+    cols_next = stat_decay * cols + column
+    moment_next = moment_decay * moment + (1.0 - moment_decay) * precond
+    update_step = moment_decay * moment_next + (1.0 - moment_decay) * precond
+    master = weight - learn_rate * update_step
+    return (master, to_bf16(master), update_step, moment_next, rows_next, cols_next)
+
+
+def gather_plan(
+    inputs,
+    query_grad,
+    forget_grad,
+    forget_pre,
+    lower_bound,
+    query_weight,
+    forget_weight,
+    query_moment,
+    forget_moment,
+    query_rows,
+    forget_rows,
+    query_cols,
+    forget_cols,
+    query_row_root,
+    forget_row_root,
+    query_col_root,
+    forget_col_root,
+):
+    sigma_gate = jax.nn.sigmoid(forget_pre.astype(jnp.float32))
+    forget_cot = to_bf16(
+        forget_grad.astype(jnp.float32) * (1.0 - lower_bound) * sigma_gate * (1.0 - sigma_gate)
+    )
+    query_outer, forget_outer, query_pre, forget_pre_out, query_column, forget_column = (
+        relayed_products(
+            inputs,
+            jnp.concatenate([query_grad, forget_cot], axis=1),
+            query_row_root,
+            forget_row_root,
+            query_col_root,
+            forget_col_root,
+        )
+    )
+    query_out = finish_update(
+        query_weight, query_moment, query_rows, query_cols, query_outer, query_pre, query_column
+    )
+    forget_out = finish_update(
+        forget_weight, forget_moment, forget_rows, forget_cols,
+        forget_outer, forget_pre_out, forget_column,
+    )
+    return tuple(piece for pair in zip(query_out, forget_out) for piece in pair)
+
+
+def on_device(*args):
+    token_count = args[0].shape[0] * lax.axis_size("fs")
+    feature_count = args[0].shape[1] * lax.axis_size("tp")
+    paired = lax.axis_size("fs") % 2 == 0 and lax.axis_size("tp") == 4
+    if paired and token_count <= feature_count:
+        return gather_plan(*args)
+    return reduce_plan(*args)
+
+
 def solution(mesh):
     in_specs = (
         P("fs", "tp"),

time: 289 us -> 80.7 us (0.28)
  waiting for transfers between devices: 211 us -> 0 us
  Pallas kernels: 0 us -> 67 us
  local copies, waits for them, and re-layouts: 18.7 us -> 0.04 us
  blocking collectives: 15.6 us -> 0 us
  matrix products: 14.9 us -> 0 us
  between operations: 15.3 us -> 0.75 us
    reduce_scatter x1 -> x0, waiting for transfers between devices: 89.6 us -> none  [on_device(): lax.psum_scatter(lax.dot_general(gathered, joined, (((0,), (0,)), ((), ()...]
    all_gather x2 -> x0, waiting for transfers between devices: 78.2 us -> none  [the longest x1 39.1 us: on_device(): lax.all_gather(gradients[0].astype(jnp.bfloat16), 'fs', axis=0, tiled=True)]
    pallas_call x0 -> x1, Pallas kernels: none -> 67 us  [relayed_products(): pl.pallas_call(relay_kernel, out_shape=[jax.ShapeDtypeStruct((chunk, feat...]
    psum x1 -> x0, waiting for transfers between devices: 42.8 us -> none  [on_device(): lax.psum(results[0][1].astype(jnp.bfloat16), 'tp').astype(jnp.float32)]
    dot_general x9 -> x0, matrix products: 14.9 us -> none  [the longest x2 5.01 us: fold_one(): lax.dot_general(grad_mine, shard_piece, (((1,), (1,)), ((), ())), precisi...]
    dot_general x2 -> x0, local copies, waits for them, and re-layouts: 9.2 us -> none  [fold_one(): jnp.einsum('rhi,rhj->hij', by_head, by_head, precision=highest)]
    all_gather x1 -> x0, blocking collectives: 8.87 us -> none  [on_device(): gathered = lax.all_gather(inputs, 'tp', axis=1, tiled=True)]
    psum x1 -> x0, blocking collectives: 6.7 us -> none  [on_device(): lax.psum(query_trace.astype(jnp.bfloat16), 'tp').astype(jnp.float32)]
  transfers between devices with their start and end apart: 4 -> 0, of which waited for: 4 -> 0; matrix products, arithmetic and copies ran while one was open for 3% -> 0% of each run, Pallas kernels for 0% -> 0%
where the time goes in v2:
time: 80.7 us; the launch traced here: 79.5 us
  Pallas kernels  67 us (83%)
  other arithmetic  11.6 us (14%)
    pallas_call x1, Pallas kernels, relayed_products(): pl.pallas_call(relay_kernel, out_shape=[jax.ShapeDtypeStruct((chunk, feat...  67 us
    add x1, other arithmetic, finish_update(): rows_next = stat_decay * rows + outer.astype(jnp.float32)  4.28 us
    convert_element_type x2, other arithmetic, to_bf16(): return value.astype(jnp.bfloat16)  3.23 us
    add x1, other arithmetic, finish_update(): cols_next = stat_decay * cols + column  1.85 us

profile of v2, /device:TPU:0, one launch (start us, length us, event | category | flops | bytes accessed | tf_op | source)
XLA Modules:
  0.0 79.5 jit_solution(16242118162428309641)
XLA Ops:
  0.6 0.0 copy-start.6
  0.7 0.0 copy-start.7
  0.7 0.0 copy-start.3
  0.7 0.0 copy-start.5
  0.7 0.0 copy-start.2
  0.7 0.0 copy-start.4
  0.7 0.8 broadcast_subtract_fusion
  1.5 0.9 %multiply_convert_fusion = bf16[128,256]{1,0:T(8,128)(2,1)S(1)} fusion(bf16[128,256]{1,0:T(8,128)(2,1)} %param.20, bf16[128,256]{1,0:T(8,128)(2,1)} %param.19, f32[256]{0:T(256)S(1)} %broadcast_subtract_fusion), kind=kLoop, calls=%fused_computation.11 | loop fusion | flops 327680 | bytes 197632 | tf_op jit(solution)/shard_map/convert_element_type | solution.py:161
  2.4 1.5 %pad_maximum_fusion.g_ref = bf16[128,512]{1,0:T(8,128)(2,1)} fusion(bf16[128,256]{1,0:T(8,128)(2,1)S(1)} %multiply_convert_fusion, bf16[128,256]{1,0:T(8,128)(2,1)} %param.18), kind=kLoop, calls=%fused_computation.8 | loop fusion | flops 262144 | bytes 262144 | tf_op jit(solution)/shard_map/concatenate | solution.py:441
  3.9 67.0 %shard_map.256 = (bf16[256,2048]{1,0:T(8,128)(2,1)}, bf16[256,2048]{1,0:T(8,128)(2,1)}, f32[256,256]{1,0:T(8,128)}, f32[256,256]{1,0:T(8,128)}, f32[2,128,128]{2,1,0:T(8,128)}, /*index=5*/f32[2,128,128]{2,1,0:T(8,128)}) custom-call(bf16[128,512]{1,0:T(8,128)(2,1)} %x_ref.1, bf16[128,512]{1,0:T(8,128)(2,1)} %pad_maximum_fusion.g_ref, ...), custom_call_target="tpu_custom_call" | custom-call | tf_op jit(solution)/shard_map/pallas_call | solution.py:378
  71.0 0.0 copy-done.6
  71.0 0.0 copy-done.7
  71.0 0.0 copy-start
  71.0 0.0 copy-start.1
  71.0 1.8 %multiply_add_fusion.4 = (f32[2,128,128]{2,1,0:T(8,128)}, f32[2,128,128]{2,1,0:T(8,128)}) fusion(f32[2,128,128]{2,1,0:T(8,128)} %get-tuple-element.23, f32[2,128,128]{2,1,0:T(8,128)S(1)} %copy-done.6, f32[2,128,128]{2,1,0:T(8,128)} %get-tuple-element.22, f32[2,128,128]{2,1,0:T(8,128)S(1)} %copy-done.7), kind=kLoop, calls=%fused_computation.9 | loop fusion | flops 131072 | bytes 786432 | tf_op jit(solution)/shard_map/add | solution.py:408
  72.9 0.0 copy-done.3
  72.9 0.0 copy-done.5
  72.9 0.0 copy-done.2
  72.9 0.0 copy-done.4
  72.9 2.3 %fusion = (bf16[256,256]{1,0:T(8,128)(2,1)}, f32[256,256]{1,0:T(8,128)}, f32[256,256]{1,0:T(8,128)}, f32[256,256]{1,0:T(8,128)}, bf16[256,256]{1,0:T(8,128)(2,1)...) fusion(f32[256,256]{1,0:T(8,128)S(1)} %copy-done.2, f32[256,256]{1,0:T(8,128)} %get-tuple-element.19, ...), kind=kLoop, calls=%fused_computation.13 | loop fusion | flops 1048576 | bytes 3407872 | tf_op jit(solution)/shard_map/convert_element_type | solution.py:161
  75.2 0.0 copy-done
  75.2 0.0 copy-done.1
  75.2 4.3 %convert_add_fusion = (f32[256,2048]{1,0:T(8,128)}, f32[256,2048]{1,0:T(8,128)}) fusion(bf16[256,2048]{1,0:T(8,128)(2,1)} %get-tuple-element.21, f32[256,2048]{1,0:T(8,128)S(1)} %copy-done, bf16[256,2048]{1,0:T(8,128)(2,1)} %get-tuple-element.20, f32[256,2048]{1,0:T(8,128)S(1)} %copy-done.1), kind=kLoop, calls=%fused_computation | loop fusion | flops 3145728 | bytes 10485760 | tf_op jit(solution)/shard_map/add | solution.py:407
Async XLA Ops:
  0.6 70.3 %copy-start.6 = (f32[2,128,128]{2,1,0:T(8,128)S(1)}, f32[2,128,128]{2,1,0:T(8,128)}, u32[]{:S(2)}) copy-start(f32[2,128,128]{2,1,0:T(8,128)} %param.29) | copy-start | bytes 393220
  0.7 70.3 %copy-start.7 = (f32[2,128,128]{2,1,0:T(8,128)S(1)}, f32[2,128,128]{2,1,0:T(8,128)}, u32[]{:S(2)}) copy-start(f32[2,128,128]{2,1,0:T(8,128)} %param.28) | copy-start | bytes 393220
  0.7 72.2 %copy-start.3 = (f32[256,256]{1,0:T(8,128)S(1)}, f32[256,256]{1,0:T(8,128)}, u32[]{:S(2)}) copy-start(f32[256,256]{1,0:T(8,128)} %param.25) | copy-start | bytes 786436
  0.7 72.2 %copy-start.5 = (f32[256,256]{1,0:T(8,128)S(1)}, f32[256,256]{1,0:T(8,128)}, u32[]{:S(2)}) copy-start(f32[256,256]{1,0:T(8,128)} %param.24) | copy-start | bytes 786436
  0.7 72.2 %copy-start.2 = (f32[256,256]{1,0:T(8,128)S(1)}, f32[256,256]{1,0:T(8,128)}, u32[]{:S(2)}) copy-start(f32[256,256]{1,0:T(8,128)} %param.23) | copy-start | bytes 786436
  0.7 72.2 %copy-start.4 = (f32[256,256]{1,0:T(8,128)S(1)}, f32[256,256]{1,0:T(8,128)}, u32[]{:S(2)}) copy-start(f32[256,256]{1,0:T(8,128)} %param.22) | copy-start | bytes 786436
  71.0 4.2 %copy-start = (f32[256,2048]{1,0:T(8,128)S(1)}, f32[256,2048]{1,0:T(8,128)}, u32[]{:S(2)}) copy-start(f32[256,2048]{1,0:T(8,128)} %param.27) | copy-start | bytes 6291460
  71.0 4.2 %copy-start.1 = (f32[256,2048]{1,0:T(8,128)S(1)}, f32[256,2048]{1,0:T(8,128)}, u32[]{:S(2)}) copy-start(f32[256,2048]{1,0:T(8,128)} %param.26) | copy-start | bytes 6291460

commit v3 on v2

--- a/solution.py
+++ b/solution.py
@@ -167,8 +167,8 @@
 
 def relay_kernel(
     x_ref, g_ref, rq_ref, rf_ref, cq_ref, cf_ref,
-    sq_ref, sf_ref, pq_ref, pf_ref, kq_ref, kf_ref,
-    xs, gs, xt, grad, left, own_sem, send_sem, recv_sem,
+    s_ref, pq_ref, pf_ref, kq_ref, kf_ref,
+    xs, gs, xt, acc, other, grad, owned, left, norms, own_sem, send_sem, recv_sem, swap_sem,
 ):
     shards = xs.shape[0]
     depth = shards // 2
@@ -211,10 +211,15 @@
     slots = (xs, gs)
     pending = []
 
-    def copy_of(kind, src, slot, name, number):
+    def place(kind, slot, half):
+        if kind == 1 and half is not None:
+            return slots[kind].at[slot[0], slot[1], half]
+        return slots[kind].at[slot[0], slot[1]]
+
+    def copy_of(kind, src, slot, name, number, half=None):
         return pltpu.make_async_remote_copy(
             src_ref=src,
-            dst_ref=slots[kind].at[slot[0], slot[1]],
+            dst_ref=place(kind, slot, half),
             send_sem=send_sem.at[number],
             recv_sem=recv_sem.at[kind, slot[0], slot[1]],
             device_id=beside[name],
@@ -223,13 +228,16 @@
 
     def send(kind, src, slot, name, cond=None):
         number = len(pending)
-        build = functools.partial(copy_of, kind, src, slot, name, number)
+        half = 1 - pc if name == "core" else None
+        if kind == 1 and half is not None:
+            src = src.at[half]
+        build = functools.partial(copy_of, kind, src, slot, name, number, half)
         guarded(cond, lambda: build().start())
         pending.append((cond, build))
 
-    def arrive(kind, slot, cond=None):
-        here = slots[kind].at[slot[0], slot[1]]
-        guarded(cond, lambda: copy_of(kind, here, slot, "core", 0).wait_recv())
+    def arrive(kind, slot, cond=None, half=None):
+        here = place(kind, slot, half)
+        guarded(cond, lambda: copy_of(kind, here, slot, "core", 0, half).wait_recv())
 
     def forward(kind, slot, names, cond=None):
         for name in names:
@@ -269,6 +277,59 @@
                 for slot in lasts(kind, layer):
                     arrive(kind, slot, cond)
                     forward(kind, slot, ("core",), cond)
+
+    width = gs.shape[4]
+    parts = gs.shape[1]
+    chunk = s_ref.shape[1]
+    steps = acc.shape[0] // chunk
+    own_lanes = pl.ds(pl.multiple_of(tp * width, width), width)
+    low = jnp.minimum(z, depth - 1 - z)
+
+    def layer_of(turn):
+        if turn == 0:
+            return z
+        near = z - (turn + 1) // 2 if turn % 2 == 1 else z + turn // 2
+        far = jnp.where(2 * z < depth, turn, depth - 1 - turn)
+        return jnp.where(turn <= 2 * low, near, far)
+
+    def multiply(turn):
+        layer = layer_of(turn)
+        for across in range(2):
+            for part in range(2):
+                slot = (2 * layer + across, 2 * part + 1 - pc)
+                for kind in range(2):
+                    arrive(kind, slot, half=pc)
+        for across in range(2):
+            for part in range(parts):
+                block_t = xs[2 * layer + across, part].T
+                xt[part * span : (part + 1) * span, across * block : (across + 1) * block] = block_t
+        first, final = turn == 0, turn == depth - 1
+        both = pl.ds(2 * layer, 2)
+
+        def step_body(step, total):
+            rows = pl.ds(pl.multiple_of(step * chunk, chunk), chunk)
+            for part in range(parts):
+                cot = gs[both, part, pc].reshape(2 * block, width)
+                piece = wide_dot(xt[rows, :], cot, ((1,), (0,)))
+                lanes = slice(part * width, (part + 1) * width)
+                if not first:
+                    piece = piece + acc[rows, lanes]
+                if final:
+                    grad[rows, lanes] = to_bf16(piece)
+                    total = total + jnp.sum(piece * piece, axis=0, keepdims=True)
+                else:
+                    acc[rows, lanes] = piece
+            cot = gs[both, tp, 1 - pc].reshape(2 * block, width)
+            piece = wide_dot(xt[rows, :], cot, ((1,), (0,)))
+            if not first:
+                piece = piece + other[rows, :]
+            if final:
+                owned[1 - pc, rows, :] = to_bf16(piece)
+            else:
+                other[rows, :] = piece
+            return total
+
+        return lax.fori_loop(0, steps, step_body, jnp.zeros((1, width), jnp.float32))
 
     previous = None
     for distance in range(depth):
@@ -296,70 +357,79 @@
                 forward(kind, slot, (orders[kind][1], "core"), cond)
         if previous is not None:
             finals(previous)
+            if distance == 1:
+                for kind in range(2):
+                    keep[kind].wait()
+            multiply(distance - 1)
         previous = stage
     finals(previous)
-    for kind in range(2):
-        keep[kind].wait()
-    for layer in range(depth):
-        for across in range(2):
-            for part in range(2):
-                slot = (2 * layer + across, 2 * part + 1 - pc)
-                for kind in range(2):
-                    arrive(kind, slot)
-
-    @pl.loop(0, shards)
-    def _(shard):
-        lanes = pl.ds(pl.multiple_of(shard * block, block), block)
-        for part in range(xs.shape[1]):
-            xt[part * span : (part + 1) * span, lanes] = xs[shard, part].T
-
-    width = gs.shape[3] // 2
-    chunk = sq_ref.shape[0]
-    steps = xt.shape[0] // chunk
-    tokens = shards * block
-    own_lanes = pl.ds(pl.multiple_of(tp * width, width), width)
-    for which, (root, col_root, outer_ref, pre_ref, col_ref) in enumerate(
-        (
-            (rq_ref, cq_ref, sq_ref, pq_ref, kq_ref),
-            (rf_ref, cf_ref, sf_ref, pf_ref, kf_ref),
-        )
-    ):
-        def multiply(step, total, which=which):
-            rows = pl.ds(pl.multiple_of(step * chunk, chunk), chunk)
-            for part in range(gs.shape[1]):
-                cot = gs[:, part, :, which * width : (which + 1) * width].reshape(tokens, width)
-                piece = wide_dot(xt[rows, :], cot, ((1,), (0,)))
-                grad[rows, part * width : (part + 1) * width] = to_bf16(piece)
-                total = total + jnp.sum(piece * piece, axis=0, keepdims=True)
-            return total
-
-        total = lax.fori_loop(0, steps, multiply, jnp.zeros((1, width), jnp.float32))
-        square = jnp.sum(total, axis=1, keepdims=True)
-        scale_twice = float(grad.shape[0] * grad.shape[1]) / (square + 1.0)
-        norm_scale = jnp.sqrt(scale_twice)
-        left[...] = jnp.zeros_like(left)
-        col_ref[...] = jnp.zeros_like(col_ref)
-        mine = pl.ds(pl.multiple_of(fs * chunk, chunk), chunk)
-
-        @pl.loop(0, steps)
-        def _(step):
-            rows = pl.ds(pl.multiple_of(step * chunk, chunk), chunk)
-            outer = wide_dot(grad[mine, :], grad[rows, :], ((1,), (1,)))
-            outer_ref[:, rows] = to_bf16(
-                outer * ((1.0 - stat_decay) / grad.shape[1] * scale_twice)
-            )
-            part = grad[rows, own_lanes]
-            left[...] += wide_dot(root[:, rows], part, ((1,), (0,)))
-            for head in range(width // HEAD):
+    total = multiply(depth - 1)
+
+    tp_core = (fs, tp + 1 - 2 * pc)
+    square = jnp.sum(total, axis=1, keepdims=True)
+    norms[0] = jnp.broadcast_to(square, norms.shape[1:])
+    swap_norm = pltpu.make_async_remote_copy(
+        src_ref=norms.at[0], dst_ref=norms.at[1],
+        send_sem=swap_sem.at[0], recv_sem=swap_sem.at[1],
+        device_id=tp_core, device_id_type=MESH,
+    )
+    swap_rows = pltpu.make_async_remote_copy(
+        src_ref=s_ref.at[pc], dst_ref=s_ref.at[pc],
+        send_sem=swap_sem.at[2], recv_sem=swap_sem.at[3],
+        device_id=tp_core, device_id_type=MESH,
+    )
+    take_rows = pltpu.make_async_remote_copy(
+        src_ref=s_ref.at[1 - pc], dst_ref=s_ref.at[1 - pc],
+        send_sem=swap_sem.at[2], recv_sem=swap_sem.at[3],
+        device_id=tp_core, device_id_type=MESH,
+    )
+    size = float(grad.shape[0] * grad.shape[1])
+    outer_scale = (1.0 - stat_decay) / grad.shape[1] * (size / (square + 1.0))
+    mine = pl.ds(pl.multiple_of(fs * chunk, chunk), chunk)
+
+    @pl.loop(0, steps)
+    def _(step):
+        rows = pl.ds(pl.multiple_of(step * chunk, chunk), chunk)
+        outer = wide_dot(grad[mine, :], grad[rows, :], ((1,), (1,)))
+        s_ref[pc, :, rows] = to_bf16(outer * outer_scale)
+        owned[pc, rows, :] = grad[rows, own_lanes]
+
+    swap_norm.start()
+    heads = width // HEAD
+    left[...] = jnp.zeros_like(left)
+    kq_ref[...] = jnp.zeros_like(kq_ref)
+    kf_ref[...] = jnp.zeros_like(kf_ref)
+    swap_rows.start()
+
+    @pl.loop(0, steps)
+    def _(step):
+        rows = pl.ds(pl.multiple_of(step * chunk, chunk), chunk)
+        for which, (root, col_ref) in enumerate(((rq_ref, kq_ref), (rf_ref, kf_ref))):
+            part = owned[which, rows, :]
+            left[which] += wide_dot(root[:, rows], part, ((1,), (0,)))
+            for head in range(heads):
                 piece = part[:, head * HEAD : (head + 1) * HEAD]
                 col_ref[head] += wide_dot(piece, piece, ((0,), (0,)))
 
-        for head in range(width // HEAD):
+    swap_norm.wait()
+    mine_sum, their_sum = norms[0, 0:1, 0:1], norms[1, 0:1, 0:1]
+    sums = (
+        jnp.where(pc == 0, mine_sum, their_sum),
+        jnp.where(pc == 0, their_sum, mine_sum),
+    )
+    for which, (col_root, pre_ref, col_ref) in enumerate(
+        ((cq_ref, pq_ref, kq_ref), (cf_ref, pf_ref, kf_ref))
+    ):
+        scale_twice = size / (sums[which] + 1.0)
+        norm_scale = jnp.sqrt(scale_twice)
+        for head in range(heads):
             lanes = slice(head * HEAD, (head + 1) * HEAD)
             col_ref[head] = col_ref[head] * ((1.0 - stat_decay) / grad.shape[0] * scale_twice)
             pre_ref[:, lanes] = norm_scale * wide_dot(
-                to_bf16(left[:, lanes]), col_root[head], ((1,), (0,))
+                to_bf16(left[which, :, lanes]), col_root[head], ((1,), (0,))
             )
+    swap_rows.wait_send()
+    take_rows.wait_recv()
 
     for cond, build in pending:
         guarded(cond, lambda build=build: build().wait_send())
@@ -368,7 +438,7 @@
 def relayed_products(x, cots, query_root, forget_root, query_col_root, forget_col_root):
     shards, parts = lax.axis_size("fs"), lax.axis_size("tp")
     block, span = x.shape
-    width = cots.shape[1] // 2
+    width = cots.shape[2]
     chunk, features = query_root.shape
     depth = shards // 2
     sends = 2 * (5 + 8 * (depth - 1) + 2 * (2 * depth - 1) + 2 * (2 * depth - 1))
@@ -378,29 +448,55 @@
     return pl.pallas_call(
         relay_kernel,
         out_shape=[
-            jax.ShapeDtypeStruct((chunk, features), jnp.bfloat16),
-            jax.ShapeDtypeStruct((chunk, features), jnp.bfloat16),
+            jax.ShapeDtypeStruct((2, chunk, features), jnp.bfloat16),
             jax.ShapeDtypeStruct((chunk, width), f32),
             jax.ShapeDtypeStruct((chunk, width), f32),
             jax.ShapeDtypeStruct(heads, f32),
             jax.ShapeDtypeStruct(heads, f32),
         ],
         in_specs=[vmem] * 6,
-        out_specs=[vmem] * 6,
+        out_specs=[vmem] * 5,
         scratch_shapes=[
             pltpu.VMEM((shards, parts, block, span), jnp.bfloat16),
-            pltpu.VMEM((shards, parts, block, 2 * width), jnp.bfloat16),
-            pltpu.VMEM((features, shards * block), jnp.bfloat16),
+            pltpu.VMEM((shards, parts, 2, block, width), jnp.bfloat16),
+            pltpu.VMEM((features, 2 * block), jnp.bfloat16),
+            pltpu.VMEM((features, parts * width), f32),
+            pltpu.VMEM((features, width), f32),
             pltpu.VMEM((features, parts * width), jnp.bfloat16),
-            pltpu.VMEM((chunk, width), f32),
+            pltpu.VMEM((2, features, width), jnp.bfloat16),
+            pltpu.VMEM((2, chunk, width), f32),
+            pltpu.VMEM((2, 8, 128), f32),
             pltpu.SemaphoreType.DMA((2,)),
             pltpu.SemaphoreType.DMA((sends,)),
             pltpu.SemaphoreType.DMA((2, shards, parts)),
+            pltpu.SemaphoreType.DMA((4,)),
         ],
         compiler_params=pltpu.CompilerParams(
-            collective_id=0, has_side_effects=True, vmem_limit_bytes=56 * 1024 * 1024
+            collective_id=0, has_side_effects=True, vmem_limit_bytes=30 * 1024 * 1024
         ),
     )(x, cots, query_root, forget_root, query_col_root, forget_col_root)
+
+
+def pack_kernel(query_ref, forget_ref, pre_ref, bound_ref, out_ref):
+    out_ref[0] = query_ref[...]
+    sigma_gate = jax.nn.sigmoid(pre_ref[...].astype(jnp.float32))
+    out_ref[1] = to_bf16(
+        forget_ref[...].astype(jnp.float32)
+        * (1.0 - bound_ref[...])
+        * sigma_gate
+        * (1.0 - sigma_gate)
+    )
+
+
+def packed_cotangents(query_grad, forget_grad, forget_pre, lower_bound):
+    vmem = pl.BlockSpec(memory_space=pltpu.VMEM)
+    return pl.pallas_call(
+        pack_kernel,
+        out_shape=jax.ShapeDtypeStruct((2,) + query_grad.shape, jnp.bfloat16),
+        in_specs=[vmem] * 4,
+        out_specs=vmem,
+        compiler_params=pltpu.CompilerParams(vmem_limit_bytes=4 * 1024 * 1024),
+    )(query_grad, forget_grad, forget_pre, lower_bound.reshape(1, -1))
 
 
 def finish_update(weight, moment, rows, cols, outer, precond, column):
@@ -431,20 +527,15 @@
     query_col_root,
     forget_col_root,
 ):
-    sigma_gate = jax.nn.sigmoid(forget_pre.astype(jnp.float32))
-    forget_cot = to_bf16(
-        forget_grad.astype(jnp.float32) * (1.0 - lower_bound) * sigma_gate * (1.0 - sigma_gate)
-    )
-    query_outer, forget_outer, query_pre, forget_pre_out, query_column, forget_column = (
-        relayed_products(
-            inputs,
-            jnp.concatenate([query_grad, forget_cot], axis=1),
-            query_row_root,
-            forget_row_root,
-            query_col_root,
-            forget_col_root,
-        )
-    )
+    outers, query_pre, forget_pre_out, query_column, forget_column = relayed_products(
+        inputs,
+        packed_cotangents(query_grad, forget_grad, forget_pre, lower_bound),
+        query_row_root,
+        forget_row_root,
+        query_col_root,
+        forget_col_root,
+    )
+    query_outer, forget_outer = outers[0], outers[1]
     query_out = finish_update(
         query_weight, query_moment, query_rows, query_cols, query_outer, query_pre, query_column
     )

time: 80.7 us -> 77.2 us (0.957)
  local copies, waits for them, and re-layouts: 0.04 us -> 9.2 us
  other arithmetic: 11.6 us -> 4.83 us
  Pallas kernels: 67 us -> 61.9 us
    unnamed x16 -> x34, local copies, waits for them, and re-layouts: 0.04 us -> 9.2 us
    pallas_call x1 -> x2, Pallas kernels: 67 us -> 61.9 us  [the longest x1 61.9 us: relayed_products(): pl.pallas_call(relay_kernel, out_shape=[jax.ShapeDtypeStruct((2, chunk, f...]
    convert_element_type x2 -> x1, other arithmetic: 3.23 us -> 1.28 us  [to_bf16(): return value.astype(jnp.bfloat16)]
    concatenate x1 -> x0, other arithmetic: 1.51 us -> none  [gather_plan(): jnp.concatenate([query_grad, forget_cot], axis=1)]
    add x1, other arithmetic: 4.28 us -> 2.82 us  [finish_update(): rows_next = stat_decay * rows + outer.astype(jnp.float32)]
    add x1, other arithmetic: 1.85 us -> 0.73 us  [finish_update(): cols_next = stat_decay * cols + column]
where the time goes in v3:
time: 77.2 us; the launch traced here: 76.7 us
  Pallas kernels  61.9 us (80%)
  local copies, waits for them, and re-layouts  9.2 us (12%)
  other arithmetic  4.83 us (6%)
    pallas_call x1, Pallas kernels, relayed_products(): pl.pallas_call(relay_kernel, out_shape=[jax.ShapeDtypeStruct((2, chunk, f...  61.9 us
    unnamed x34, local copies, waits for them, and re-layouts  9.2 us
    add x1, other arithmetic, finish_update(): rows_next = stat_decay * rows + outer.astype(jnp.float32)  2.82 us

profile of v3, /device:TPU:0, one launch (start us, length us, event | category | flops | bytes accessed | tf_op | source)
XLA Modules:
  0.0 76.7 jit_solution(4117096759207834117)
XLA Ops:
  0.6 0.0 copy-start.3
  0.7 0.8 %copy-done.3 = bf16[128,256]{1,0:T(8,128)(2,1)S(1)} copy-done((bf16[128,256]{1,0:T(8,128)(2,1)S(1)}, bf16[128,256]{1,0:T(8,128)(2,1)}, u32[]{:S(2)}) %copy-start.3) | copy-done | bytes 65560
  1.5 0.0 copy-start.4
  1.5 0.8 %copy-done.4 = bf16[128,256]{1,0:T(8,128)(2,1)S(1)} copy-done((bf16[128,256]{1,0:T(8,128)(2,1)S(1)}, bf16[128,256]{1,0:T(8,128)(2,1)}, u32[]{:S(2)}) %copy-start.4) | copy-done | bytes 65560
  2.3 0.0 copy-start.5
  2.3 0.8 %copy-done.5 = bf16[128,256]{1,0:T(8,128)(2,1)S(1)} copy-done((bf16[128,256]{1,0:T(8,128)(2,1)S(1)}, bf16[128,256]{1,0:T(8,128)(2,1)}, u32[]{:S(2)}) %copy-start.5) | copy-done | bytes 65560
  3.2 0.0 copy-start.8
  3.2 0.7 copy-done.8
  3.8 0.0 copy-start.11
  3.9 0.0 copy-start
  3.9 1.2 %copy-done = bf16[256,2048]{1,0:T(8,128)(2,1)S(1)} copy-done((bf16[256,2048]{1,0:T(8,128)(2,1)S(1)}, bf16[256,2048]{1,0:T(8,128)(2,1)}, u32[]{:S(2)}) %copy-start) | copy-done | bytes 1048600
  5.2 0.0 copy-start.1
  5.2 1.2 %copy-done.1 = bf16[256,2048]{1,0:T(8,128)(2,1)S(1)} copy-done((bf16[256,2048]{1,0:T(8,128)(2,1)S(1)}, bf16[256,2048]{1,0:T(8,128)(2,1)}, u32[]{:S(2)}) %copy-start.1) | copy-done | bytes 1048600
  6.4 0.0 copy-start.2
  6.4 0.9 %copy-done.2 = bf16[128,512]{1,0:T(8,128)(2,1)S(1)} copy-done((bf16[128,512]{1,0:T(8,128)(2,1)S(1)}, bf16[128,512]{1,0:T(8,128)(2,1)}, u32[]{:S(2)}) %copy-start.2) | copy-done | bytes 131096
  7.3 0.8 %copy-done.6 = bf16[2,128,128]{2,1,0:T(8,128)(2,1)S(1)} copy-done((bf16[2,128,128]{2,1,0:T(8,128)(2,1)S(1)}, bf16[2,128,128]{2,1,0:T(8,128)(2,1)}, u32[]{:S(2)}) %copy-start.6) | copy-done | bytes 65560
  8.1 0.8 %copy-done.7 = bf16[2,128,128]{2,1,0:T(8,128)(2,1)S(1)} copy-done((bf16[2,128,128]{2,1,0:T(8,128)(2,1)S(1)}, bf16[2,128,128]{2,1,0:T(8,128)(2,1)}, u32[]{:S(2)}) %copy-start.7) | copy-done | bytes 65560
  9.0 0.0 copy-start.14
  9.0 61.9 %shard_map.257 = (bf16[2,256,2048]{2,1,0:T(8,128)(2,1)S(1)}, f32[256,256]{1,0:T(8,128)S(1)}, f32[256,256]{1,0:T(8,128)S(1)}, f32[2,128,128]{2,1,0:T(8,128)S(1)}, f32[2,128,128]{2,1,0:T(8,128)S(1)}) custom-call(bf16[128,512]{1,0:T(8,128)(2,1)S(1)} %copy-done.2, bf16[2,128,256]{2,1,0:T(8,128)(2,1)S(1)} %shard_map.256.g_ref, bf16[256,2048]{1,0:T(8,128)(2,1)S(1)} %copy-done, ...), custom_call_target="tpu_custom_call" | custom-call | tf_op jit(solution)/shard_map/pallas_call | solution.py:448
  70.9 0.0 copy-done.15
  70.9 0.0 copy-done.16
  70.9 0.0 copy-start.9
  70.9 0.0 copy-start.10
  70.9 0.7 multiply_add_fusion.4
  71.7 0.0 copy-done.11
  71.7 0.0 copy-done.12
  71.7 0.0 copy-done.13
  71.7 0.0 copy-done.14
  71.7 1.3 %fusion = (bf16[256,256]{1,0:T(8,128)(2,1)}, f32[256,256]{1,0:T(8,128)}, f32[256,256]{1,0:T(8,128)}, f32[256,256]{1,0:T(8,128)}, bf16[256,256]{1,0:T(8,128)(2,1)...) fusion(f32[256,256]{1,0:T(8,128)S(1)} %copy-done.11, f32[256,256]{1,0:T(8,128)S(1)} %get-tuple-element.18, ...), kind=kLoop, calls=%fused_computation.10 | loop fusion | flops 1048576 | bytes 3407872 | tf_op jit(solution)/shard_map/convert_element_type | solution.py:161
  73.0 0.0 copy-done.9
  73.0 0.9 %copy-done.10 = f32[256,2048]{1,0:T(8,128)S(1)} copy-done((f32[256,2048]{1,0:T(8,128)S(1)}, f32[256,2048]{1,0:T(8,128)}, u32[]{:S(2)}) %copy-start.10) | copy-done | bytes 2097176
  73.9 2.8 %convert_add_fusion = (f32[256,2048]{1,0:T(8,128)}, f32[256,2048]{1,0:T(8,128)}) fusion(f32[256,2048]{1,0:T(8,128)S(1)} %copy-done.9, bf16[2,256,2048]{2,1,0:T(8,128)(2,1)S(1)} %get-tuple-element.19, f32[256,2048]{1,0:T(8,128)S(1)} %copy-done.10), kind=kLoop, calls=%fused_computation | loop fusion | flops 3145728 | bytes 10485760 | tf_op jit(solution)/shard_map/add | solution.py:503
  (7 shorter events, 0.1 us)
Async XLA Ops:
  0.6 0.8 %copy-start.3 = (bf16[128,256]{1,0:T(8,128)(2,1)S(1)}, bf16[128,256]{1,0:T(8,128)(2,1)}, u32[]{:S(2)}) copy-start(bf16[128,256]{1,0:T(8,128)(2,1)} %query_ref.1) | copy-start | bytes 196612
  1.5 0.8 %copy-start.4 = (bf16[128,256]{1,0:T(8,128)(2,1)S(1)}, bf16[128,256]{1,0:T(8,128)(2,1)}, u32[]{:S(2)}) copy-start(bf16[128,256]{1,0:T(8,128)(2,1)} %forget_ref.1) | copy-start | bytes 196612
  2.3 0.8 %copy-start.5 = (bf16[128,256]{1,0:T(8,128)(2,1)S(1)}, bf16[128,256]{1,0:T(8,128)(2,1)}, u32[]{:S(2)}) copy-start(bf16[128,256]{1,0:T(8,128)(2,1)} %pre_ref.1) | copy-start | bytes 196612
  3.2 0.7 copy-start.8
  3.8 67.8 %copy-start.11 = (f32[256,256]{1,0:T(8,128)S(1)}, f32[256,256]{1,0:T(8,128)}, u32[]{:S(2)}) copy-start(f32[256,256]{1,0:T(8,128)} %param.23) | copy-start | bytes 786436
  3.9 1.3 %copy-start = (bf16[256,2048]{1,0:T(8,128)(2,1)S(1)}, bf16[256,2048]{1,0:T(8,128)(2,1)}, u32[]{:S(2)}) copy-start(bf16[256,2048]{1,0:T(8,128)(2,1)} %rq_ref.1) | copy-start | bytes 3145732
  5.2 1.2 %copy-start.1 = (bf16[256,2048]{1,0:T(8,128)(2,1)S(1)}, bf16[256,2048]{1,0:T(8,128)(2,1)}, u32[]{:S(2)}) copy-start(bf16[256,2048]{1,0:T(8,128)(2,1)} %rf_ref.1) | copy-start | bytes 3145732
  6.4 0.9 %copy-start.2 = (bf16[128,512]{1,0:T(8,128)(2,1)S(1)}, bf16[128,512]{1,0:T(8,128)(2,1)}, u32[]{:S(2)}) copy-start(bf16[128,512]{1,0:T(8,128)(2,1)} %x_ref.1) | copy-start | bytes 393220
  7.3 0.8 %copy-start.6 = (bf16[2,128,128]{2,1,0:T(8,128)(2,1)S(1)}, bf16[2,128,128]{2,1,0:T(8,128)(2,1)}, u32[]{:S(2)}) copy-start(bf16[2,128,128]{2,1,0:T(8,128)(2,1)} %cq_ref.1) | copy-start | bytes 196612
  8.1 0.8 %copy-start.7 = (bf16[2,128,128]{2,1,0:T(8,128)(2,1)S(1)}, bf16[2,128,128]{2,1,0:T(8,128)(2,1)}, u32[]{:S(2)}) copy-start(bf16[2,128,128]{2,1,0:T(8,128)(2,1)} %cf_ref.1) | copy-start | bytes 196612
  9.0 61.9 %copy-start.15 = (f32[2,128,128]{2,1,0:T(8,128)S(1)}, f32[2,128,128]{2,1,0:T(8,128)}, u32[]{:S(2)}) copy-start(f32[2,128,128]{2,1,0:T(8,128)} %param.29) | copy-start | bytes 393220
  9.0 61.9 %copy-start.16 = (f32[2,128,128]{2,1,0:T(8,128)S(1)}, f32[2,128,128]{2,1,0:T(8,128)}, u32[]{:S(2)}) copy-start(f32[2,128,128]{2,1,0:T(8,128)} %param.28) | copy-start | bytes 393220
  9.0 62.7 %copy-start.12 = (f32[256,256]{1,0:T(8,128)S(1)}, f32[256,256]{1,0:T(8,128)}, u32[]{:S(2)}) copy-start(f32[256,256]{1,0:T(8,128)} %param.25) | copy-start | bytes 786436
  9.0 62.7 %copy-start.13 = (f32[256,256]{1,0:T(8,128)S(1)}, f32[256,256]{1,0:T(8,128)}, u32[]{:S(2)}) copy-start(f32[256,256]{1,0:T(8,128)} %param.22) | copy-start | bytes 786436
  9.0 62.7 %copy-start.14 = (f32[256,256]{1,0:T(8,128)S(1)}, f32[256,256]{1,0:T(8,128)}, u32[]{:S(2)}) copy-start(f32[256,256]{1,0:T(8,128)} %param.24) | copy-start | bytes 786436
  70.9 2.1 %copy-start.9 = (f32[256,2048]{1,0:T(8,128)S(1)}, f32[256,2048]{1,0:T(8,128)}, u32[]{:S(2)}) copy-start(f32[256,2048]{1,0:T(8,128)} %param.27) | copy-start | bytes 6291460
  70.9 3.0 %copy-start.10 = (f32[256,2048]{1,0:T(8,128)S(1)}, f32[256,2048]{1,0:T(8,128)}, u32[]{:S(2)}) copy-start(f32[256,2048]{1,0:T(8,128)} %param.26) | copy-start | bytes 6291460

commit v4 on v3

--- a/solution.py
+++ b/solution.py
@@ -166,9 +166,9 @@
 
 
 def relay_kernel(
-    x_ref, g_ref, rq_ref, rf_ref, cq_ref, cf_ref,
+    x_ref, g_ref, rq_hbm, rf_hbm, cq_ref, cf_ref,
     s_ref, pq_ref, pf_ref, kq_ref, kf_ref,
-    xs, gs, xt, acc, other, grad, owned, left, norms, own_sem, send_sem, recv_sem, swap_sem,
+    xs, gs, xt, acc, other, grad, owned, left, norms, roots, own_sem, send_sem, recv_sem, swap_sem,
 ):
     shards = xs.shape[0]
     depth = shards // 2
@@ -261,6 +261,10 @@
         pltpu.make_async_copy(sources[kind], slots[kind].at[fs, tp], own_sem.at[kind])
         for kind in range(2)
     ]
+    loads = [
+        pltpu.make_async_copy(source, roots.at[which], own_sem.at[2 + which])
+        for which, source in enumerate((rq_hbm, rf_hbm))
+    ]
     for kind in range(2):
         send(kind, sources[kind], own, "up", has_up)
         send(kind, sources[kind], own, "down", has_down)
@@ -270,6 +274,7 @@
         send(kind, sources[kind], own, orders[kind][1])
         send(kind, sources[kind], own, "core")
         keep[kind].start()
+        loads[kind].start()
 
     def finals(stage):
         for layer, cond in stage:
@@ -331,38 +336,44 @@
 
         return lax.fori_loop(0, steps, step_body, jnp.zeros((1, width), jnp.float32))
 
-    previous = None
-    for distance in range(depth):
-        stage = []
+    def layers_at(distance):
         if distance == 0:
-            stage.append((z, None))
-        else:
-            stage.append((z - distance, z >= distance))
-            stage.append((z + distance, z + distance < depth))
-            for sign, (layer, cond) in zip((-1, 1), stage):
-                for kind in range(2):
-                    slot = (2 * layer + px, tp)
-                    arrive(kind, slot, cond)
-                    if sign < 0:
-                        onward, onto = "up", jnp.logical_and(cond, has_up)
-                    else:
-                        onward, onto = "down", jnp.logical_and(cond, has_down)
-                    if distance < depth - 1:
-                        forward(kind, slot, (onward,), onto)
-                    forward(kind, slot, orders[kind] + ("core",), cond)
-        for layer, cond in stage:
+            return ((z, None),)
+        return (
+            (z - distance, z >= distance),
+            (z + distance, z + distance < depth),
+        )
+
+    def along(distance):
+        for onward, (layer, cond), more in zip(
+            ("up", "down"), layers_at(distance), (has_up, has_down)
+        ):
+            for kind in range(2):
+                slot = (2 * layer + px, tp)
+                arrive(kind, slot, cond)
+                if distance < depth - 1:
+                    forward(kind, slot, (onward,), jnp.logical_and(cond, more))
+                forward(kind, slot, orders[kind] + ("core",), cond)
+
+    def across_pair(distance):
+        for layer, cond in layers_at(distance):
             for kind in range(2):
                 slot = crossed(kind, layer)
                 arrive(kind, slot, cond)
                 forward(kind, slot, (orders[kind][1], "core"), cond)
-        if previous is not None:
-            finals(previous)
-            if distance == 1:
-                for kind in range(2):
-                    keep[kind].wait()
-            multiply(distance - 1)
-        previous = stage
-    finals(previous)
+
+    for distance in range(1, depth):
+        along(distance)
+        across_pair(distance - 1)
+    finals(layers_at(0))
+    for kind in range(2):
+        keep[kind].wait()
+    multiply(0)
+    across_pair(depth - 1)
+    for distance in range(1, depth - 1):
+        finals(layers_at(distance))
+        multiply(distance)
+    finals(layers_at(depth - 1))
     total = multiply(depth - 1)
 
     tp_core = (fs, tp + 1 - 2 * pc)
@@ -400,11 +411,13 @@
     kq_ref[...] = jnp.zeros_like(kq_ref)
     kf_ref[...] = jnp.zeros_like(kf_ref)
     swap_rows.start()
+    for load in loads:
+        load.wait()
 
     @pl.loop(0, steps)
     def _(step):
         rows = pl.ds(pl.multiple_of(step * chunk, chunk), chunk)
-        for which, (root, col_ref) in enumerate(((rq_ref, kq_ref), (rf_ref, kf_ref))):
+        for which, (root, col_ref) in enumerate(((roots.at[0], kq_ref), (roots.at[1], kf_ref))):
             part = owned[which, rows, :]
             left[which] += wide_dot(root[:, rows], part, ((1,), (0,)))
             for head in range(heads):
@@ -445,6 +458,7 @@
     f32 = jnp.float32
     heads = query_col_root.shape
     vmem = pl.BlockSpec(memory_space=pltpu.VMEM)
+    hbm = pl.BlockSpec(memory_space=pltpu.HBM)
     return pl.pallas_call(
         relay_kernel,
         out_shape=[
@@ -454,7 +468,7 @@
             jax.ShapeDtypeStruct(heads, f32),
             jax.ShapeDtypeStruct(heads, f32),
         ],
-        in_specs=[vmem] * 6,
+        in_specs=[vmem, vmem, hbm, hbm, vmem, vmem],
         out_specs=[vmem] * 5,
         scratch_shapes=[
             pltpu.VMEM((shards, parts, block, span), jnp.bfloat16),
@@ -466,13 +480,14 @@
             pltpu.VMEM((2, features, width), jnp.bfloat16),
             pltpu.VMEM((2, chunk, width), f32),
             pltpu.VMEM((2, 8, 128), f32),
-            pltpu.SemaphoreType.DMA((2,)),
+            pltpu.VMEM((2, chunk, features), jnp.bfloat16),
+            pltpu.SemaphoreType.DMA((4,)),
             pltpu.SemaphoreType.DMA((sends,)),
             pltpu.SemaphoreType.DMA((2, shards, parts)),
             pltpu.SemaphoreType.DMA((4,)),
         ],
         compiler_params=pltpu.CompilerParams(
-            collective_id=0, has_side_effects=True, vmem_limit_bytes=30 * 1024 * 1024
+            collective_id=0, has_side_effects=True, vmem_limit_bytes=61 * 1024 * 1024
         ),
     )(x, cots, query_root, forget_root, query_col_root, forget_col_root)
 
@@ -495,17 +510,52 @@
         out_shape=jax.ShapeDtypeStruct((2,) + query_grad.shape, jnp.bfloat16),
         in_specs=[vmem] * 4,
         out_specs=vmem,
-        compiler_params=pltpu.CompilerParams(vmem_limit_bytes=4 * 1024 * 1024),
+        compiler_params=pltpu.CompilerParams(vmem_limit_bytes=61 * 1024 * 1024),
     )(query_grad, forget_grad, forget_pre, lower_bound.reshape(1, -1))
 
 
-def finish_update(weight, moment, rows, cols, outer, precond, column):
-    rows_next = stat_decay * rows + outer.astype(jnp.float32)
-    cols_next = stat_decay * cols + column
-    moment_next = moment_decay * moment + (1.0 - moment_decay) * precond
-    update_step = moment_decay * moment_next + (1.0 - moment_decay) * precond
-    master = weight - learn_rate * update_step
-    return (master, to_bf16(master), update_step, moment_next, rows_next, cols_next)
+def finish_kernel(outer_ref, *refs):
+    pres, columns, weights, moments, rows, cols = (refs[2 * k : 2 * k + 2] for k in range(6))
+    outs = refs[12:]
+    for which in range(2):
+        master_ref, copy_ref, step_ref, moment_ref, rows_ref, cols_ref = outs[which::2]
+        precond = pres[which][...]
+        moment_next = moment_decay * moments[which][...] + (1.0 - moment_decay) * precond
+        update_step = moment_decay * moment_next + (1.0 - moment_decay) * precond
+        master = weights[which][...] - learn_rate * update_step
+        master_ref[...] = master
+        copy_ref[...] = to_bf16(master)
+        step_ref[...] = update_step
+        moment_ref[...] = moment_next
+        rows_ref[...] = stat_decay * rows[which][...] + outer_ref[which].astype(jnp.float32)
+        cols_ref[...] = stat_decay * cols[which][...] + columns[which][...]
+
+
+def finished(outers, pres, columns, weights, moments, rows, cols):
+    f32, bf16 = jnp.float32, jnp.bfloat16
+    chunk, width = weights[0].shape
+    features = rows[0].shape[1]
+    heads = cols[0].shape
+    steps = 4
+    tile = chunk // steps
+    narrow = pl.BlockSpec((tile, width), lambda i: (i, 0))
+    wide = pl.BlockSpec((tile, features), lambda i: (i, 0))
+    head = pl.BlockSpec((heads[0], heads[1] // steps, heads[2]), lambda i: (0, i, 0))
+    both = pl.BlockSpec((2, tile, features), lambda i: (0, i, 0))
+    flat = lambda kind: [jax.ShapeDtypeStruct((chunk, width), kind)] * 2
+    return pl.pallas_call(
+        finish_kernel,
+        grid=(steps,),
+        out_shape=flat(f32)
+        + flat(bf16)
+        + flat(f32)
+        + flat(f32)
+        + [jax.ShapeDtypeStruct((chunk, features), f32)] * 2
+        + [jax.ShapeDtypeStruct(heads, f32)] * 2,
+        in_specs=[both] + [narrow] * 2 + [head] * 2 + [narrow] * 4 + [wide] * 2 + [head] * 2,
+        out_specs=[narrow] * 8 + [wide] * 2 + [head] * 2,
+        compiler_params=pltpu.CompilerParams(vmem_limit_bytes=61 * 1024 * 1024),
+    )(outers, *pres, *columns, *weights, *moments, *rows, *cols)
 
 
 def gather_plan(
@@ -535,15 +585,17 @@
         query_col_root,
         forget_col_root,
     )
-    query_outer, forget_outer = outers[0], outers[1]
-    query_out = finish_update(
-        query_weight, query_moment, query_rows, query_cols, query_outer, query_pre, query_column
-    )
-    forget_out = finish_update(
-        forget_weight, forget_moment, forget_rows, forget_cols,
-        forget_outer, forget_pre_out, forget_column,
-    )
-    return tuple(piece for pair in zip(query_out, forget_out) for piece in pair)
+    return tuple(
+        finished(
+            outers,
+            (query_pre, forget_pre_out),
+            (query_column, forget_column),
+            (query_weight, forget_weight),
+            (query_moment, forget_moment),
+            (query_rows, forget_rows),
+            (query_cols, forget_cols),
+        )
+    )
 
 
 def on_device(*args):

time: 77.2 us -> 67 us (0.87)
  local copies, waits for them, and re-layouts: 9.2 us -> 0 us
  other arithmetic: 4.83 us -> 0 us
  Pallas kernels: 61.9 us -> 65.9 us
    unnamed x34 -> x0, local copies, waits for them, and re-layouts: 9.2 us -> none
    pallas_call x0 -> x1, Pallas kernels: none -> 6.19 us  [finished(): pl.pallas_call(finish_kernel, grid=(steps,), out_shape=flat(f32) + flat(b...]
    pallas_call x1, Pallas kernels: 61.9 us -> 58.1 us  [relayed_products(): pl.pallas_call(relay_kernel, out_shape=[jax.ShapeDtypeStruct((2, chunk, f...]
    add x2 -> x0, other arithmetic: 3.55 us -> none  [the longest x1 2.82 us: finish_update(): rows_next = stat_decay * rows + outer.astype(jnp.float32)]
    pallas_call x1, Pallas kernels: 0.05 us -> 1.61 us  [packed_cotangents(): pl.pallas_call(pack_kernel, out_shape=jax.ShapeDtypeStruct((2,) + query_g...]
    convert_element_type x1 -> x0, other arithmetic: 1.28 us -> none  [to_bf16(): return value.astype(jnp.bfloat16)]
where the time goes in v4:
time: 67 us; the launch traced here: 66.6 us
  Pallas kernels  65.9 us (98%)
    pallas_call x1, Pallas kernels, relayed_products(): pl.pallas_call(relay_kernel, out_shape=[jax.ShapeDtypeStruct((2, chunk, f...  58.1 us
    pallas_call x1, Pallas kernels, finished(): pl.pallas_call(finish_kernel, grid=(steps,), out_shape=flat(f32) + flat(b...  6.19 us
    pallas_call x1, Pallas kernels, packed_cotangents(): pl.pallas_call(pack_kernel, out_shape=jax.ShapeDtypeStruct((2,) + query_g...  1.61 us

profile of v4, /device:TPU:0, one launch (start us, length us, event | category | flops | bytes accessed | tf_op | source)
XLA Modules:
  0.0 66.6 jit_solution(11509846063053629115)
XLA Ops:
  0.6 1.6 %shard_map.256.g_ref = bf16[2,128,256]{2,1,0:T(8,128)(2,1)} custom-call(bf16[128,256]{1,0:T(8,128)(2,1)} %query_ref.1, bf16[128,256]{1,0:T(8,128)(2,1)} %forget_ref.1, bf16[128,256]{1,0:T(8,128)(2,1)} %pre_ref.1, f32[1,256]{1,0:T(1,128)} %bitcast.1), custom_call_target="tpu_custom_call" | custom-call | tf_op jit(solution)/shard_map/pallas_call | solution.py:508
  2.3 58.1 %shard_map.257 = (bf16[2,256,2048]{2,1,0:T(8,128)(2,1)}, f32[256,256]{1,0:T(8,128)}, f32[256,256]{1,0:T(8,128)}, f32[2,128,128]{2,1,0:T(8,128)}, f32[2,128,128]{2,1,0:T(8,128)}) custom-call(bf16[128,512]{1,0:T(8,128)(2,1)} %x_ref.1, bf16[2,128,256]{2,1,0:T(8,128)(2,1)} %shard_map.256.g_ref, bf16[256,2048]{1,0:T(8,128)(2,1)} %rq_hbm.1, ...), custom_call_target="tpu_custom_call" | custom-call | tf_op jit(solution)/shard_map/pallas_call | solution.py:462
  60.4 6.2 %shard_map.258 = (f32[256,256]{1,0:T(8,128)}, f32[256,256]{1,0:T(8,128)}, bf16[256,256]{1,0:T(8,128)(2,1)}, bf16[256,256]{1,0:T(8,128)(2,1)}, f32[256,256]{1,0:T...) custom-call(bf16[2,256,2048]{2,1,0:T(8,128)(2,1)} %get-tuple-element, ...), custom_call_target="tpu_custom_call" | custom-call | tf_op jit(solution)/shard_map/pallas_call | solution.py:546

commit v5 on v4

--- a/solution.py
+++ b/solution.py
@@ -364,11 +364,13 @@
 
     for distance in range(1, depth):
         along(distance)
-        across_pair(distance - 1)
+        if distance < depth - 1:
+            across_pair(distance - 1)
     finals(layers_at(0))
     for kind in range(2):
         keep[kind].wait()
     multiply(0)
+    across_pair(depth - 2)
     across_pair(depth - 1)
     for distance in range(1, depth - 1):
         finals(layers_at(distance))
@@ -536,7 +538,7 @@
     chunk, width = weights[0].shape
     features = rows[0].shape[1]
     heads = cols[0].shape
-    steps = 4
+    steps = 2
     tile = chunk // steps
     narrow = pl.BlockSpec((tile, width), lambda i: (i, 0))
     wide = pl.BlockSpec((tile, features), lambda i: (i, 0))

time: 67 us -> 66.3 us (0.990)
  no operation moved by 1% of the time
where the time goes in v5:
time: 66.3 us; the launch traced here: 65.9 us
  Pallas kernels  65.3 us (98%)
    pallas_call x1, Pallas kernels, relayed_products(): pl.pallas_call(relay_kernel, out_shape=[jax.ShapeDtypeStruct((2, chunk, f...  58.1 us
    pallas_call x1, Pallas kernels, finished(): pl.pallas_call(finish_kernel, grid=(steps,), out_shape=flat(f32) + flat(b...  5.55 us
    pallas_call x1, Pallas kernels, packed_cotangents(): pl.pallas_call(pack_kernel, out_shape=jax.ShapeDtypeStruct((2,) + query_g...  1.61 us

profile of v5, /device:TPU:0, one launch (start us, length us, event | category | flops | bytes accessed | tf_op | source)
XLA Modules:
  0.0 65.9 jit_solution(7214577012157983288)
XLA Ops:
  0.6 1.6 %shard_map.256.g_ref = bf16[2,128,256]{2,1,0:T(8,128)(2,1)} custom-call(bf16[128,256]{1,0:T(8,128)(2,1)} %query_ref.1, bf16[128,256]{1,0:T(8,128)(2,1)} %forget_ref.1, bf16[128,256]{1,0:T(8,128)(2,1)} %pre_ref.1, f32[1,256]{1,0:T(1,128)} %bitcast.1), custom_call_target="tpu_custom_call" | custom-call | tf_op jit(solution)/shard_map/pallas_call | solution.py:510
  2.3 58.1 %shard_map.257 = (bf16[2,256,2048]{2,1,0:T(8,128)(2,1)}, f32[256,256]{1,0:T(8,128)}, f32[256,256]{1,0:T(8,128)}, f32[2,128,128]{2,1,0:T(8,128)}, f32[2,128,128]{2,1,0:T(8,128)}) custom-call(bf16[128,512]{1,0:T(8,128)(2,1)} %x_ref.1, bf16[2,128,256]{2,1,0:T(8,128)(2,1)} %shard_map.256.g_ref, bf16[256,2048]{1,0:T(8,128)(2,1)} %rq_hbm.1, ...), custom_call_target="tpu_custom_call" | custom-call | tf_op jit(solution)/shard_map/pallas_call | solution.py:464
  60.4 5.5 %shard_map.258 = (f32[256,256]{1,0:T(8,128)}, f32[256,256]{1,0:T(8,128)}, bf16[256,256]{1,0:T(8,128)(2,1)}, bf16[256,256]{1,0:T(8,128)(2,1)}, f32[256,256]{1,0:T...) custom-call(bf16[2,256,2048]{2,1,0:T(8,128)(2,1)} %get-tuple-element, ...), custom_call_target="tpu_custom_call" | custom-call | tf_op jit(solution)/shard_map/pallas_call | solution.py:548
